TPU v7x, 256 devices: a 4x2x16 block of a 4x16x16 slice. The times are simulated.
256 devices in a mesh: grp: 2 (over y), sp: 16 (over z), tp: 8 (over x, core).
Axes of the slice: x: 4, y: 2, z: 16, core: 2. Of those that a mesh axis runs over, the one named last changes fastest.
The devices are a block of a 4x16x16 slice.
Arguments:
- queries: bfloat16 [32768, 1024], P(('grp', 'sp'), 'tp'), parts along dimension 0, may hold values from -6 to 6
- keys: bfloat16 [32768, 256], P(('grp', 'sp')), parts along dimension 0, may hold values from -6 to 6
- values: bfloat16 [32768, 256], P(('grp', 'sp')), parts along dimension 0, may hold values from -6 to 6
- query_gain: float32 [128], replicated, may hold values from 1.2 to 6, as said below
- key_gain: float32 [128], replicated, may hold values from 1.2 to 6, as said below
- out_weight: bfloat16 [1024, 2048], replicated, may hold values from -6 to 6
- residual_in: bfloat16 [32768, 2048], P(('grp', 'sp', 'tp')), parts along dimension 0, may hold values from -6 to 6
- norm_gain: float32 [2048], replicated, may hold values from 0.1 to 1.9
- gate_weight: bfloat16 [2048, 2816], P('sp', 'tp'), may hold values from -0.125 to 0.125
- up_weight: bfloat16 [2048, 2816], P('sp', 'tp'), may hold values from -0.125 to 0.125
- down_weight: bfloat16 [2816, 2048], P('tp', 'sp'), may hold values from -0.109375 to 0.109375
Outputs:
- layer_out: bfloat16 [32768, 2048], P(('grp', 'sp', 'tp')), parts along dimension 0
There are 2 independent parts, one for each index of `grp`. A program takes and returns all parts, laid end to end along the dimension named above; an argument that names none is the same for every part. Nothing has to cross between parts.
Inputs may be any that keep to these rules, and one draw needn't show every extreme that they name: `query_gain`: positive gains. `key_gain`: positive gains.
All inputs are finite; a program needn't handle non-finite values.
Results may differ from a plain program's by a relative error of at most 0.015.
The roundings to bfloat16 on the way count: a program that leaves them out, or rounds other values in their place, can miss the bound.
Values may be sent and summed in bfloat16 or wider, within the bound.
A program may use at most 128 MiB of HBM per device.

v0:
```python
import jax
import jax.numpy as jnp
from jax import lax
from jax.sharding import PartitionSpec as P

HQ = 8
KV = 2
HD = 128
GRID_W = 64


def gather_turned(arrays, axis, dims):
    turned = [jnp.moveaxis(a, dim, 0) for a, dim in zip(arrays, dims)]
    both = jnp.concatenate([t.reshape(len(t), -1) for t in turned], axis=1)
    result, at, gathered = (lax.all_gather(both, axis, axis=0, tiled=True), 0, [])
    for t, dim in zip(turned, dims):
        section = result[:, at : at + t[0].size].reshape(-1, *t.shape[1:])
        gathered.append(jnp.moveaxis(section, 0, dim))
        at += t[0].size
    return tuple(gathered)


def sent_together(arrays, axis, dim, along):
    ends, at = ([], 0)
    for a in arrays[:-1]:
        at += a.shape[along]
        ends.append(at)
    both = jnp.concatenate(arrays, axis=along)
    return tuple(jnp.split(lax.all_gather(both, axis, axis=dim, tiled=True), ends, axis=along))


def rotate(widened, positions):
    half = HD // 2
    inverse = 10000.0 ** (-jnp.arange(0, half, 2, dtype=jnp.float32) / half)
    grid_row = (positions // GRID_W).astype(jnp.float32)
    grid_col = (positions % GRID_W).astype(jnp.float32)
    angles = jnp.concatenate(
        [grid_row[:, None] * inverse[None], grid_col[:, None] * inverse[None]], axis=-1
    )
    cosine = jnp.cos(angles)[:, None, :]
    sine = jnp.sin(angles)[:, None, :]
    pairs = widened.reshape(widened.shape[0], widened.shape[1], half, 2)
    first = pairs[..., 0]
    second = pairs[..., 1]
    turned = jnp.stack([first * cosine - second * sine, first * sine + second * cosine], axis=-1)
    return turned.reshape(widened.shape)


def prepare(source, gain, positions, heads):
    widened = source.astype(jnp.float32).reshape(source.shape[0], heads, HD)
    widened = (
        widened * lax.rsqrt(jnp.mean(widened * widened, axis=-1, keepdims=True) + 1e-06) * gain
    )
    return rotate(widened, positions).astype(jnp.bfloat16)


def local(
    queries,
    keys,
    values,
    query_gain,
    key_gain,
    out_weight,
    residual_in,
    norm_gain,
    gate_weight,
    up_weight,
    down_weight,
):
    tok_rows = queries.shape[0]
    heads_here = queries.shape[1] // HD
    full_gate, full_up, full_down = gather_turned(
        (gate_weight, up_weight, down_weight), "sp", (0, 0, 1)
    )
    seq_index = lax.axis_index("sp")
    head_index = lax.axis_index("tp")
    positions = seq_index * tok_rows + jnp.arange(tok_rows, dtype=jnp.int32)
    query_rot = prepare(queries, query_gain, positions, heads_here)
    query_rot = query_rot.transpose(1, 0, 2).reshape(heads_here * tok_rows, HD)
    pair_index = head_index * heads_here // (HQ // KV)
    key_block = lax.dynamic_slice_in_dim(keys, pair_index * HD, HD, 1)
    value_block = lax.dynamic_slice_in_dim(values, pair_index * HD, HD, 1)
    key_rot = prepare(key_block, key_gain, positions, 1).reshape(tok_rows, HD)
    scale = HD ** (-0.5)

    def attend_block(carry, block):
        running_max, denominator, weighted = carry
        key_part, value_part = block
        scores = (
            lax.dot_general(
                query_rot, key_part, (((1,), (1,)), ((), ())), preferred_element_type=jnp.float32
            )
            * scale
        )
        new_max = jnp.maximum(running_max, jnp.max(scores, axis=1))
        factor = jnp.exp(running_max - new_max)
        raised = jnp.exp(scores - new_max[:, None])
        denominator = denominator * factor + jnp.sum(raised, axis=1)
        weighted = weighted * factor[:, None] + jnp.dot(
            raised.astype(jnp.bfloat16), value_part, preferred_element_type=jnp.float32
        )
        return ((new_max, denominator, weighted), None)

    start_carry = (
        jnp.full((heads_here * tok_rows,), -1e30, jnp.float32),
        jnp.zeros((heads_here * tok_rows,), jnp.float32),
        jnp.zeros((heads_here * tok_rows, HD), jnp.float32),
    )
    carry = start_carry
    pieces = sent_together((key_rot, value_block), "sp", 0, 1)
    length = pieces[0].shape[0]
    block = tok_rows
    count = length // block
    key_parts = pieces[0].reshape(count, block, HD)
    value_parts = pieces[1].reshape(count, block, HD)
    carry, unused = lax.scan(attend_block, carry, (key_parts, value_parts))
    running_max, denominator, weighted = carry
    attended = (weighted / denominator[:, None]).astype(jnp.bfloat16)
    attended = (
        attended.reshape(heads_here, tok_rows, HD)
        .transpose(1, 0, 2)
        .reshape(tok_rows, heads_here * HD)
    )
    traded = lax.all_to_all(attended, "tp", split_axis=0, concat_axis=1, tiled=True)
    projected = jnp.dot(traded, out_weight, preferred_element_type=jnp.float32)
    middle = residual_in.astype(jnp.float32) + projected
    normed = (
        middle * lax.rsqrt(jnp.mean(middle * middle, axis=-1, keepdims=True) + 1e-06) * norm_gain
    )
    normed = normed.astype(jnp.bfloat16)
    rows_all = lax.all_gather(normed, "tp", axis=0, tiled=True)
    gate_act = jnp.dot(rows_all, full_gate, preferred_element_type=jnp.float32)
    up_act = jnp.dot(rows_all, full_up, preferred_element_type=jnp.float32)
    hidden = (jax.nn.silu(gate_act) * up_act).astype(jnp.bfloat16)
    mixer_out = lax.psum_scatter(
        jnp.dot(hidden, full_down, preferred_element_type=jnp.float32).astype(jnp.bfloat16),
        "tp",
        scatter_dimension=0,
        tiled=True,
    ).astype(jnp.float32)
    return (middle + mixer_out).astype(jnp.bfloat16)


def solution(mesh):
    placed = (
        P(("grp", "sp"), "tp"),
        P(("grp", "sp"), None),
        P(("grp", "sp"), None),
        P(),
        P(),
        P(),
        P(("grp", "sp", "tp"), None),
        P(),
        P("sp", "tp"),
        P("sp", "tp"),
        P("tp", "sp"),
    )
    return jax.shard_map(
        local, mesh=mesh, in_specs=placed, out_specs=P(("grp", "sp", "tp"), None), check_vma=False
    )
```

profile of v0, /device:TPU:33, one launch (start us, length us, event | category | flops | bytes accessed | tf_op | source)
XLA Modules:
  0.0 412.4 jit_solution(15702451741075299920)
XLA Ops:
  17.6 117.0 %all-gather.4.cloned.1.call-done = bf16[16384,256]{0,1:T(8,128)(2,1)} async-done(((bf16[1024,256]{0,1:T(8,128)(2,1)}), bf16[16384,256]{0,1:T(8,128)(2,1)}) %all-gather.4.cloned.1.call-update) | async-done | bytes 8388624 | tf_op jit(solution)/shard_map/all_gather | solution.py:29
  134.6 5.8 %fusion.42 = (bf16[16384,128]{0,1:T(8,128)(2,1)}, bf16[16384,128]{0,1:T(8,128)(2,1)}) fusion(bf16[16384,256]{0,1:T(8,128)(2,1)} %all-gather.4.cloned.1.call-done), kind=kLoop, calls=%fused_computation.75 | loop fusion | bytes 16777216 | tf_op jit(solution)/shard_map/split | solution.py:29
  140.4 6.4 %copy.41 = bf16[16384,128]{1,0:T(8,128)(2,1)} copy(bf16[16384,128]{0,1:T(8,128)(2,1)} %get-tuple-element.109) | data formatting | bytes 8388608
  146.8 6.4 %copy.42 = bf16[16384,128]{1,0:T(8,128)(2,1)} copy(bf16[16384,128]{0,1:T(8,128)(2,1)} %get-tuple-element.108) | data formatting | bytes 8388608
  153.2 144.5 %while.15 = (s32[]{:T(128)}, f32[1024]{0:T(1024)S(1)}, f32[1024]{0:T(1024)S(1)}, f32[1024,128]{1,0:T(8,128)S(1)}, bf16[16,1024,128]{2,1,0:T(8,128)(2,1)}, /*inde...) while((s32[]{:T(128)}, f32[1024]{0:T(1024)S(1)}, ...), condition=%wide.region_5.6_spmd.clone, body=%wide.region_2.5_spmd.clone.sunk | while | flops 545657856 | bytes 31261828 | solution.py:116
  153.2 3.6 multiply_reduce_fusion.3
  162.3 3.6 multiply_reduce_fusion.3
  180.4 3.6 multiply_reduce_fusion.3
  189.5 3.6 multiply_reduce_fusion.3
  198.6 3.6 multiply_reduce_fusion.3
  207.6 3.6 multiply_reduce_fusion.3
  216.7 3.6 multiply_reduce_fusion.3
  225.7 3.6 multiply_reduce_fusion.3
  234.7 3.6 multiply_reduce_fusion.3
  243.7 3.6 multiply_reduce_fusion.3
  252.7 3.6 multiply_reduce_fusion.3
  261.7 3.6 multiply_reduce_fusion.3
  270.7 3.6 multiply_reduce_fusion.3
  279.7 3.6 multiply_reduce_fusion.3
  298.0 11.4 %all_to_all.19 = bf16[8,128,128]{2,1,0:T(8,128)(2,1)S(1)} all-to-all(bf16[8,128,128]{2,1,0:T(8,128)(2,1)S(1)} %bitcast.40), channel_id=1, replica_groups=mesh['grp'=2,'sp'=16,'tp'=8] {'tp'}, dimensions={0} | all-to-all | bytes 524288 | tf_op jit(solution)/shard_map/all_to_all | solution.py:124
  313.9 35.1 %all-gather.6.cloned.1.call-done = bf16[1024,2048]{1,0:T(8,128)(2,1)} async-done(((bf16[128,2048]{1,0:T(8,128)(2,1)}), bf16[1024,2048]{1,0:T(8,128)(2,1)}) %all-gather.6.cloned.1.call-update) | async-done | bytes 4194320 | tf_op jit(solution)/shard_map/all_gather | solution.py:131
  349.0 4.3 %fusion.20 = f32[1024,352]{0,1:T(8,128)S(1)} fusion(bf16[1024,2048]{1,0:T(8,128)(2,1)} %all-gather.6.cloned.1.call-done, bf16[2048,1056]{0,1:T(8,128)(2,1)} %all-gather.8.cloned.1.call-done), kind=kOutput, calls=%fused_computation.26 | convolution fusion | flops 1476395008 | bytes 7077888 | tf_op jit(solution)/shard_map/dot_general | solution.py:132
  353.3 9.0 %convolution_convert_fusion = bf16[1024,2048]{1,0:T(8,128)(2,1)} fusion(bf16[2048,1056]{0,1:T(8,128)(2,1)} %all-gather.8.cloned.1.call-done, bf16[1024,2048]{1,0:T(8,128)(2,1)} %all-gather.6.cloned.1.call-done, f32[1024,352]{0,1:T(8,128)S(1)} %fusion.20), kind=kOutput, calls=%fused_computation.21 | convolution fusion | flops 2957049856 | bytes 12713984 | tf_op jit(solution)/shard_map/dot_general | solution.py:136
  362.4 41.5 %reduce-scatter.2.cloned.1.call-done = bf16[128,2048]{1,0:T(8,128)(2,1)} async-done(((bf16[1024,2048]{1,0:T(8,128)(2,1)}), bf16[128,2048]{1,0:T(8,128)(2,1)}) %reduce-scatter.2.cloned.1.call-update) | async-done | bytes 524304 | tf_op jit(solution)/shard_map/reduce_scatter | solution.py:135
  (170 shorter events, 111.2 us)
Async XLA Ops:
  6.5 8.3 %copy-start = (bf16[1024,256]{1,0:T(8,128)(2,1)S(1)}, bf16[1024,256]{1,0:T(8,128)(2,1)}, u32[]{:S(2)}) copy-start(bf16[1024,256]{1,0:T(8,128)(2,1)} %param.15) | copy-start | bytes 1572868
  6.6 128.0 %all-gather.4.cloned.1.call-start = ((), (), s32[]{:S(2)}) async-start(), calls=%async_computation.2 | async-start | bytes 8912896 | tf_op jit(solution)/shard_map/all_gather | solution.py:29
  12.4 3.7 copy-start.3
  12.4 3.7 copy-start.4
  12.4 3.7 copy-start.5
  16.0 297.9 %all-gather.8.cloned.1.call-start = ((), (), s32[]{:S(2)}) async-start(), calls=%async_computation.4 | async-start | bytes 4595712 | tf_op jit(solution)/shard_map/all_gather | solution.py:15
  16.9 332.1 %all-gather.6.cloned.1.call-start = ((), (), s32[]{:S(2)}) async-start(), calls=%async_computation.3 | async-start | bytes 4718592 | tf_op jit(solution)/shard_map/all_gather | solution.py:131
  153.2 156.4 %copy-start.2 = (bf16[128,2048]{1,0:T(8,128)(2,1)S(1)}, bf16[128,2048]{1,0:T(8,128)(2,1)}, u32[]{:S(2)}) copy-start(bf16[128,2048]{1,0:T(8,128)(2,1)} %param.19) | copy-start | bytes 1572868
  156.8 3.5 copy-start.1
  165.9 3.5 copy-start.1
  175.0 3.5 copy-start.1
  184.0 3.5 copy-start.1
  193.1 3.5 copy-start.1
  202.2 3.5 copy-start.1
  211.2 3.5 copy-start.1
  220.3 3.4 copy-start.1
  229.3 3.4 copy-start.1
  238.3 3.4 copy-start.1
  247.3 3.4 copy-start.1
  256.3 3.4 copy-start.1
  265.3 3.4 copy-start.1
  292.3 3.4 copy-start.1
  297.7 14.9 %copy-start.6 = (f32[2048]{0:T(1024)S(1)}, f32[2048]{0:T(1024)}, u32[]{:S(2)}) copy-start(f32[2048]{0:T(1024)} %param.20) | copy-start | bytes 24580
  313.6 90.2 %reduce-scatter.2.cloned.1.call-start = ((), (), s32[]{:S(2)}) async-start(), calls=%async_computation.5 | async-start | bytes 4718592 | tf_op jit(solution)/shard_map/reduce_scatter | solution.py:135
  (2 other events, 6.9 us)
Sparse Core Ops, SparseCore 0:
  16.1 118.4 all-gather.3
  136.3 80.9 all-gather.7
  313.8 35.1 all-gather.5
  362.5 41.3 reduce-scatter.1
where the time goes:
time: 415 us; the launch traced here: 412 us
  waiting for transfers between devices  194 us (47%)
  matrix products  105 us (25%)
  other arithmetic  60.3 us (15%)
  local copies, waits for them, and re-layouts  27.6 us (7%)
  between operations  13.5 us (3%)
  blocking collectives  11.4 us (3%)
    all_gather x1, waiting for transfers between devices, sent_together(): lax.all_gather(both, axis, axis=dim, tiled=True)  117 us
    dot_general x16, matrix products, attend_block(): lax.dot_general(query_rot, key_part, (((1,), (1,)), ((), ())), preferred_...  57.4 us
    reduce_sum x16, other arithmetic, attend_block(): denominator = denominator * factor + jnp.sum(raised, axis=1)  49.4 us
    reduce_scatter x1, waiting for transfers between devices, local(): lax.psum_scatter(jnp.dot(hidden, full_down, preferred_element_type=jnp.fl...  41.5 us
    all_gather x1, waiting for transfers between devices, local(): rows_all = lax.all_gather(normed, 'tp', axis=0, tiled=True)  35.1 us
    dot_general x16, matrix products, attend_block(): jnp.dot(raised.astype(jnp.bfloat16), value_part, preferred_element_type=j...  31.1 us
    unnamed x16, local copies, waits for them, and re-layouts  13.1 us
    all_to_all x1, blocking collectives, local(): lax.all_to_all(attended, 'tp', split_axis=0, concat_axis=1, tiled=True)  11.4 us
  transfers between devices with their start and end apart: 4, of which 3 were waited for; matrix products, arithmetic and copies ran while one was open for 39% of the time, Pallas kernels for 0%

commit v1 on v0

v1 whole, which is shorter than its diff:
```python
import functools
import math

import jax
import jax.numpy as jnp
from jax import lax
from jax.experimental import pallas as pl
from jax.experimental.pallas import tpu as pltpu
from jax.sharding import PartitionSpec as P

HQ = 8
KV = 2
HD = 128
GRID_W = 64
MESH = pl.DeviceIdType.MESH
F32 = jnp.float32
BF16 = jnp.bfloat16
ROWS_ATT = 256
ROWS_FF = 256


def layer_kernel(
    n,
    n_tp,
    q_ref,
    k_ref,
    v_ref,
    qg_ref,
    kg_ref,
    inv_ref,
    ow_hbm,
    res_ref,
    ng_ref,
    gate_ref,
    up_ref,
    down_ref,
    out_ref,
    kv,
    qrot,
    acc,
    mx,
    ls,
    cosr,
    sinr,
    gw,
    uw,
    dw,
    ow,
    res,
    att,
    nrm,
    mid,
    hid,
    part,
    d2s,
    d2r,
    s1s,
    s1r,
    s2s,
    s2r,
    yk,
    zk,
    ow_sem,
    kv_ss,
    kv_rs,
    kd_ss,
    kd_rs,
    w_ss,
    w_rs,
    a_ss,
    a_rs,
    r_ss,
    r_rs,
    t_ss,
    t_rs,
):
    me = lax.axis_index("sp")
    tp = lax.axis_index("tp")
    core = lax.rem(tp, 2)
    x = tp // 2
    tok = q_ref.shape[0]
    d = res_ref.shape[1]
    own_rows = res_ref.shape[0]
    half_n = n // 2
    kv_head = tp // (n_tp // KV)

    def wrap(i):
        return lax.rem(i + n, n)

    right = wrap(me + 1)
    left = wrap(me - 1)
    n1x = x + 1 - 2 * lax.rem(x, 2)
    n2x = 3 - x
    dgx = 3 - n1x
    mate = x * 2 + 1 - core
    n1 = n1x * 2 + core
    n2 = n2x * 2 + core
    dg = dgx * 2 + core
    to_right, to_left = {"sp": right}, {"sp": left}
    to_mate, to_n1, to_n2 = {"tp": mate}, {"tp": n1}, {"tp": n2}

    def remote(src, dst, ss, rs, dev):
        return pltpu.make_async_remote_copy(
            src_ref=src, dst_ref=dst, send_sem=ss, recv_sem=rs, device_id=dev, device_id_type=MESH
        )

    load_ow = pltpu.make_async_copy(ow_hbm, ow, ow_sem)
    load_ow.start()

    barrier = pltpu.get_barrier_semaphore()
    for dev in (to_right, to_left, to_mate, to_n1, to_n2):
        pl.semaphore_signal(barrier, inc=1, device_id=dev, device_id_type=MESH)

    grid_rows = tok // GRID_W
    lane = lax.broadcasted_iota(jnp.int32, (GRID_W, HD), 1)
    row_pos = (me * grid_rows + lax.broadcasted_iota(jnp.int32, (grid_rows, HD), 0)).astype(F32)
    row_ang = row_pos * inv_ref[...]
    cosr[...] = jnp.cos(row_ang)
    sinr[...] = jnp.sin(row_ang)
    col_ang = lax.broadcasted_iota(jnp.int32, (GRID_W, HD), 0).astype(F32) * inv_ref[...]
    cos_col = jnp.cos(col_ang)
    sin_col = jnp.sin(col_ang)
    even = lax.rem(lane, 2) == 0
    by_row = lane < HD // 2

    def turned(source, gain, i):
        v = source.astype(F32)
        v = v * lax.rsqrt(jnp.mean(v * v, axis=-1, keepdims=True) + 1e-06) * gain
        cosine = jnp.where(by_row, cosr[pl.ds(i, 1), :], cos_col)
        sine = jnp.where(by_row, sinr[pl.ds(i, 1), :], sin_col)
        swapped = jnp.where(even, pltpu.roll(v, HD - 1, 1), pltpu.roll(v, 1, 1))
        signed = jnp.where(even, -sine, sine)
        return (v * cosine + swapped * signed).astype(BF16)

    kv_lanes = pl.ds(pl.multiple_of(kv_head * HD, HD), HD)

    def prep_k(i, _):
        rows = pl.ds(pl.multiple_of(i * GRID_W, GRID_W), GRID_W)
        kv[me, rows, 0:HD] = turned(k_ref[rows, kv_lanes], kg_ref[...], i)
        kv[me, rows, HD : 2 * HD] = v_ref[rows, kv_lanes]
        return 0

    lax.fori_loop(0, grid_rows, prep_k, 0)
    pl.semaphore_wait(barrier, 5)

    quarter = tok // 4
    slab = tok // 2

    def q_slot(b, a, c):
        return kv.at[b, pl.ds(pl.multiple_of((2 * a + c) * quarter, quarter), quarter), :]

    def kv_ring(direction, t, a):
        b = wrap(me - t) if direction == 0 else wrap(me + t)
        s = q_slot(b, a, core)
        return remote(
            s, s, kv_ss.at[direction, t, a], kv_rs.at[direction, t, a], (to_right, to_left)[direction]
        )

    def kv_send(direction, t, a):
        b = wrap(me - t) if direction == 0 else wrap(me + t)
        s = q_slot(b, a, core)
        return remote(
            s,
            s,
            kv_ss.at[direction, t, a],
            kv_rs.at[direction, t + 1, a],
            (to_right, to_left)[direction],
        )

    def kv_mate(direction, t, a, whose):
        b = wrap(me - t) if direction == 0 else wrap(me + t)
        s = q_slot(b, a, whose)
        return remote(s, s, kd_ss.at[direction, t, a], kd_rs.at[direction, t, a], to_mate)

    for a in range(2):
        for direction in range(2):
            kv_send(direction, 0, a).start()

    half_d = d // 2

    def res_slot(j, h=None):
        rows = pl.ds(pl.multiple_of(j * own_rows, own_rows), own_rows)
        if h is None:
            return res.at[rows, :]
        return res.at[rows, h * half_d : (h + 1) * half_d]

    def att_slot(j, h=None):
        lanes = pl.ds(pl.multiple_of(j * HD, HD), HD)
        if h is None:
            return att.at[:, lanes]
        return att.at[h * slab : (h + 1) * slab, lanes]

    def gather_steps(slot, ss, rs):
        def pair(s, i, dev):
            return remote(s, s, ss.at[i], rs.at[i], dev)

        def own(side, h):
            return pair(slot(tp, h), side * 2 + h, (to_n1, to_n2)[side])

        def arrived(side, h):
            return pair(slot((n1, n2)[side], h), side * 2 + h, (to_n1, to_n2)[side])

        def onward(h):
            return pair(slot((n1, n2)[h], h), 4 + h, (to_n2, to_n1)[h])

        def diag_arrived(h):
            return pair(slot(dg, h), 4 + h, (to_n2, to_n1)[h])

        def mates(i, j):
            return pair(slot(j), 6 + i, to_mate)

        def mate_arrived(i, j):
            return pair(slot(j + 1 - 2 * core), 6 + i, to_mate)

        def first():
            for h in (0, 1):
                own(0, h).start()
                own(1, 1 - h).start()
            mates(0, tp).start()

        def second():
            for side, h in ((0, 0), (1, 1), (0, 1), (1, 0)):
                arrived(side, h).wait_recv()
                if side == h:
                    onward(h).start()
            mates(1, n1).start()
            mates(2, n2).start()

        def third():
            diag_arrived(0).wait_recv()
            diag_arrived(1).wait_recv()
            mates(3, dg).start()

        def fourth():
            for i, j in enumerate((tp, n1, n2, dg)):
                mate_arrived(i, j).wait_recv()

        def sent():
            for side in (0, 1):
                for h in (0, 1):
                    own(side, h).wait_send()
            for h in (0, 1):
                onward(h).wait_send()
            for i, j in enumerate((tp, n1, n2, dg)):
                mates(i, j).wait_send()

        return first, second, third, fourth, sent

    res_first, res_second, res_third, res_fourth, res_sent = gather_steps(res_slot, r_ss, r_rs)
    att_first, att_second, att_third, att_fourth, att_sent = gather_steps(att_slot, a_ss, a_rs)

    gk = gate_ref.shape[0]
    ff = down_ref.shape[0]

    def w_slot(which, b):
        if which == 2:
            return dw.at[pl.ds(pl.multiple_of(b * ff, ff), ff), :]
        return (gw, uw)[which].at[pl.ds(pl.multiple_of(b * gk, gk), gk), :]

    def w_copy(which, direction, t, late):
        b = wrap(me - t) if direction == 0 else wrap(me + t)
        s = w_slot(which, b)
        return remote(
            s,
            s,
            w_ss.at[which, direction, t],
            w_rs.at[which, direction, t + late],
            (to_right, to_left)[direction],
        )

    def w_start(whiches):
        for which in whiches:
            for direction in range(2):
                w_copy(which, direction, 0, 1).start()

    def w_step(whiches, t):
        for direction in range(2):
            for which in whiches:
                w_copy(which, direction, t, 0).wait_recv()

                @pl.when((t < half_n - 1) | (core == direction))
                def _():
                    w_copy(which, direction, t, 1).start()

    def w_last(whiches):
        for direction in range(2):

            @pl.when(core == direction)
            def _():
                for which in whiches:
                    w_copy(which, direction, half_n, 0).wait_recv()

    def w_sent(whiches):
        def one(t, _):
            for direction in range(2):
                for which in whiches:

                    @pl.when((t < half_n - 1) | (core == direction))
                    def _():
                        w_copy(which, direction, t, 1).wait_send()

            return 0

        lax.fori_loop(0, half_n, one, 0)

    def prep_q(i, _):
        rows = pl.ds(pl.multiple_of(i * GRID_W, GRID_W), GRID_W)
        qrot[rows, :] = turned(q_ref[rows, :], qg_ref[...], i)
        return 0

    lax.fori_loop(0, grid_rows, prep_q, 0)
    res_slot(tp)[...] = res_ref[...]
    w_slot(0, me)[...] = gate_ref[...]
    w_slot(1, me)[...] = up_ref[...]
    w_slot(2, me)[...] = down_ref[...]
    mx[...] = jnp.full(mx.shape, -1e30, F32)
    ls[...] = jnp.zeros(ls.shape, F32)
    acc[...] = jnp.zeros(acc.shape, F32)

    factor = HD ** (-0.5) * math.log2(math.e)

    def attend(b1, h1, b2, h2):
        def one(i, _):
            rows = pl.ds(pl.multiple_of(i * ROWS_ATT, ROWS_ATT), ROWS_ATT)
            q = qrot[rows, :]
            r1 = pl.ds(pl.multiple_of(h1 * slab, slab), slab)
            r2 = pl.ds(pl.multiple_of(h2 * slab, slab), slab)
            dims = (((1,), (1,)), ((), ()))
            scores = [
                lax.dot_general(q, kv[b, r, 0:HD], dims, preferred_element_type=F32)
                for b, r in ((b1, r1), (b2, r2))
            ]
            top = None
            for s in scores:
                for j in range(slab // HD):
                    tile = s[:, j * HD : (j + 1) * HD]
                    top = tile if top is None else jnp.maximum(top, tile)
            old = mx[rows, :]
            new = jnp.maximum(old, jnp.max(top, axis=1, keepdims=True))
            mx[rows, :] = new
            alpha = jnp.exp2((old - new) * factor)
            base = new[:, 0:1]
            total = ls[rows, :] * alpha
            weighted = acc[rows, :] * alpha
            for s, (b, r) in zip(scores, ((b1, r1), (b2, r2))):
                raised = jnp.exp2((s - base) * factor)
                for j in range(slab // HD):
                    total = total + raised[:, j * HD : (j + 1) * HD]
                weighted = weighted + jnp.dot(
                    raised.astype(BF16), kv[b, r, HD : 2 * HD], preferred_element_type=F32
                )
            ls[rows, :] = total
            acc[rows, :] = weighted
            return 0

        lax.fori_loop(0, tok // ROWS_ATT, one, 0)

    def kv_take(t, a):
        for direction in range(2):
            kv_ring(direction, t, a).wait_recv()

            @pl.when((t < half_n - 1) | (core == direction))
            def _():
                kv_send(direction, t, a).start()

            kv_mate(direction, t, a, core).start()

    def mate_take(t, a):
        for direction in range(2):
            kv_mate(direction, t, a, 1 - core).wait_recv()

    kv_take(1, 0)
    res_first()
    attend(me, 0, me, 1)

    def phase(p, _):
        t, a = (p + 1) // 2, lax.rem(p + 1, 2)
        tb, ab = p // 2, lax.rem(p, 2)
        kv_take(t, a)

        @pl.when(p == 6)
        def _():
            res_second()

        @pl.when(p == 10)
        def _():
            res_third()

        @pl.when(p == 2 * half_n - 2)
        def _():
            w_start((0, 1))

        mate_take(tb, ab)
        attend(wrap(me - tb), ab, wrap(me + tb), ab)
        return 0

    lax.fori_loop(2, 2 * half_n - 1, phase, 0)
    for direction in range(2):

        @pl.when(core == direction)
        def _():
            for a in range(2):
                kv_ring(direction, half_n, a).wait_recv()
                kv_mate(direction, half_n, a, core).start()

    mate_take(half_n - 1, 1)
    attend(wrap(me - half_n + 1), 1, wrap(me + half_n - 1), 1)
    w_step((0, 1), 1)
    for direction in range(2):

        @pl.when(core == 1 - direction)
        def _():
            for a in range(2):
                kv_mate(direction, half_n, a, 1 - core).wait_recv()

    attend(wrap(me + half_n), 0, wrap(me + half_n), 1)

    def finish(i, _):
        rows = pl.ds(pl.multiple_of(i * ROWS_ATT, ROWS_ATT), ROWS_ATT)
        below = jnp.sum(ls[rows, :], axis=1, keepdims=True)
        att[rows, pl.ds(pl.multiple_of(tp * HD, HD), HD)] = (acc[rows, :] / below).astype(BF16)
        return 0

    lax.fori_loop(0, tok // ROWS_ATT, finish, 0)
    w_step((0, 1), 2)
    att_first()
    res_fourth()
    load_ow.wait()
    att_second()
    w_step((0, 1), 3)
    att_third()
    att_fourth()

    def project(i, _):
        rows = pl.ds(pl.multiple_of(i * ROWS_FF, ROWS_FF), ROWS_FF)
        middle = res[rows, :].astype(F32) + jnp.dot(
            att[rows, :], ow[...], preferred_element_type=F32
        )
        scale = lax.rsqrt(jnp.mean(middle * middle, axis=-1, keepdims=True) + 1e-06)
        nrm[rows, :] = (middle * scale * ng_ref[...]).astype(BF16)
        held = ROWS_FF // own_rows
        for j in range(held):

            @pl.when(tp == i * held + j)
            def _():
                mid[...] = middle[j * own_rows : (j + 1) * own_rows, :]

        @pl.when(i + 4 < half_n)
        def _():
            w_step((0, 1), i + 4)

        return 0

    lax.fori_loop(0, tok // ROWS_FF, project, 0)
    w_start((2,))
    w_last((0, 1))

    def units(i, _):
        rows = pl.ds(pl.multiple_of(i * ROWS_FF, ROWS_FF), ROWS_FF)
        n_rows = nrm[rows, :]
        gate = jnp.dot(n_rows, gw[...], preferred_element_type=F32)
        up = jnp.dot(n_rows, uw[...], preferred_element_type=F32)
        hid[rows, :] = (gate / (1.0 + jnp.exp(-gate)) * up).astype(BF16)

        @pl.when(i == 1)
        def _():
            w_step((2,), 1)

        @pl.when(i == 3)
        def _():
            w_step((2,), 2)

        return 0

    lax.fori_loop(0, tok // ROWS_FF, units, 0)

    near = (n1x, n2x)
    far = (n2x, n1x)
    to_near = (to_n1, to_n2)
    to_far = (to_n2, to_n1)

    def col_block(g, k):
        return wrap(me - k) if g == 0 else wrap(me + k + 1)

    def d2_copy(g, k):
        return remote(d2s.at[g, k], d2r.at[g, k], t_ss.at[0, g, k], t_rs.at[0, g, k], to_mate)

    def s1_copy(g, k):
        return remote(s1s.at[g, k], s1r.at[g, k], t_ss.at[1, g, k], t_rs.at[1, g, k], to_near[g])

    def s2_copy(g, k):
        return remote(s2s.at[g, k], s2r.at[g, k], t_ss.at[2, g, k], t_rs.at[2, g, k], to_far[g])

    def stage0(k):
        for g in range(2):
            b = col_block(g, k)
            part[g, lax.rem(k, 2)] = jnp.dot(
                hid[...],
                dw[pl.ds(pl.multiple_of(b * ff, ff), ff), :],
                preferred_element_type=F32,
            )
            for c in range(4):
                at = pl.ds(pl.multiple_of((c * 2 + 1 - core) * own_rows, own_rows), own_rows)
                d2s[g, k, c * own_rows : (c + 1) * own_rows, :] = part[g, lax.rem(k, 2), at, :].astype(
                    BF16
                )
            d2_copy(g, k).start()

    def stage1(k):
        slot = lax.rem(k, 2)
        for g in range(2):
            d2_copy(g, k).wait_recv()

            def summed(c):
                mine = pl.ds(pl.multiple_of((c * 2 + core) * own_rows, own_rows), own_rows)
                theirs = pl.ds(pl.multiple_of(c * own_rows, own_rows), own_rows)
                return part[g, slot, mine, :] + d2r[g, k, theirs, :].astype(F32)

            s1s[g, k, 0:own_rows, :] = summed(near[g]).astype(BF16)
            s1s[g, k, own_rows : 2 * own_rows, :] = summed(dgx).astype(BF16)
            yk[g, slot, 0] = summed(x)
            yk[g, slot, 1] = summed(far[g])
            s1_copy(g, k).start()

    def stage2(k):
        slot = lax.rem(k, 2)
        for g in range(2):
            s1_copy(g, k).wait_recv()
            s2s[g, k] = (
                yk[g, slot, 1] + s1r[g, k, own_rows : 2 * own_rows, :].astype(F32)
            ).astype(BF16)
            zk[g, slot] = yk[g, slot, 0] + s1r[g, k, 0:own_rows, :].astype(F32)
            s2_copy(g, k).start()

    def stage3(k):
        slot = lax.rem(k, 2)
        for g in range(2):
            s2_copy(g, k).wait_recv()
            lanes = pl.ds(pl.multiple_of(col_block(g, k) * HD, HD), HD)
            out_ref[:, lanes] = (mid[:, lanes] + zk[g, slot] + s2r[g, k].astype(F32)).astype(BF16)

    def columns(k, _):
        @pl.when(k >= 3)
        def _():
            stage3(k - 3)

        @pl.when((k >= 2) & (k < half_n + 2))
        def _():
            stage2(k - 2)

        @pl.when((k >= 1) & (k < half_n + 1))
        def _():
            stage1(k - 1)

        @pl.when(k < half_n)
        def _():
            stage0(k)

        @pl.when(k + 3 < half_n)
        def _():
            w_step((2,), k + 3)

        @pl.when(k + 3 == half_n)
        def _():
            w_last((2,))

        return 0

    lax.fori_loop(0, half_n + 3, columns, 0)

    def kv_sent(t, _):
        for a in range(2):
            for direction in range(2):

                @pl.when((t < half_n - 1) | (core == direction))
                def _():
                    kv_send(direction, t, a).wait_send()

                @pl.when(t > 0)
                def _():
                    kv_mate(direction, t, a, core).wait_send()

        return 0

    lax.fori_loop(0, half_n, kv_sent, 0)
    for direction in range(2):

        @pl.when(core == direction)
        def _():
            for a in range(2):
                kv_mate(direction, half_n, a, core).wait_send()

    w_sent((0, 1, 2))
    res_sent()
    att_sent()

    def sums_sent(k, _):
        for g in range(2):
            d2_copy(g, k).wait_send()
            s1_copy(g, k).wait_send()
            s2_copy(g, k).wait_send()
        return 0

    lax.fori_loop(0, half_n, sums_sent, 0)


def local(
    n,
    n_tp,
    queries,
    keys,
    values,
    query_gain,
    key_gain,
    out_weight,
    residual_in,
    norm_gain,
    gate_weight,
    up_weight,
    down_weight,
):
    tok = queries.shape[0]
    own_rows, d = residual_in.shape
    ff = down_weight.shape[0]
    gk = gate_weight.shape[0]
    half = HD // 2
    half_n = n // 2
    inverse = 10000.0 ** (-jnp.arange(0, half, 2, dtype=F32) / half)
    inverse = jnp.tile(jnp.repeat(inverse, 2), 2)[None]
    vmem = pl.BlockSpec(memory_space=pltpu.VMEM)
    dma = pltpu.SemaphoreType.DMA
    scratch = [
        pltpu.VMEM((n, tok, 2 * HD), BF16),
        pltpu.VMEM((tok, HD), BF16),
        pltpu.VMEM((tok, HD), F32),
        pltpu.VMEM((tok, HD), F32),
        pltpu.VMEM((tok, HD), F32),
        pltpu.VMEM((tok // GRID_W, HD), F32),
        pltpu.VMEM((tok // GRID_W, HD), F32),
        pltpu.VMEM((n * gk, ff), BF16),
        pltpu.VMEM((n * gk, ff), BF16),
        pltpu.VMEM((n * ff, HD), BF16),
        pltpu.VMEM(out_weight.shape, BF16),
        pltpu.VMEM((tok, d), BF16),
        pltpu.VMEM((tok, HQ * HD), BF16),
        pltpu.VMEM((tok, d), BF16),
        pltpu.VMEM((own_rows, d), F32),
        pltpu.VMEM((tok, ff), BF16),
        pltpu.VMEM((2, 2, tok, HD), F32),
        pltpu.VMEM((2, half_n, tok // 2, HD), BF16),
        pltpu.VMEM((2, half_n, tok // 2, HD), BF16),
        pltpu.VMEM((2, half_n, 2 * own_rows, HD), BF16),
        pltpu.VMEM((2, half_n, 2 * own_rows, HD), BF16),
        pltpu.VMEM((2, half_n, own_rows, HD), BF16),
        pltpu.VMEM((2, half_n, own_rows, HD), BF16),
        pltpu.VMEM((2, 2, 2, own_rows, HD), F32),
        pltpu.VMEM((2, 2, own_rows, HD), F32),
        dma,
        dma((2, half_n + 1, 2)),
        dma((2, half_n + 1, 2)),
        dma((2, half_n + 1, 2)),
        dma((2, half_n + 1, 2)),
        dma((3, 2, half_n + 1)),
        dma((3, 2, half_n + 1)),
        dma((10,)),
        dma((10,)),
        dma((10,)),
        dma((10,)),
        dma((3, 2, half_n)),
        dma((3, 2, half_n)),
    ]
    specs = [vmem] * 12
    specs[6] = pl.BlockSpec(memory_space=pl.ANY)
    return pl.pallas_call(
        functools.partial(layer_kernel, n, n_tp),
        out_shape=jax.ShapeDtypeStruct((own_rows, d), BF16),
        in_specs=specs,
        out_specs=vmem,
        scratch_shapes=scratch,
        compiler_params=pltpu.CompilerParams(
            collective_id=0, has_side_effects=True, vmem_limit_bytes=67043328
        ),
        name="layer",
    )(
        queries,
        keys,
        values,
        query_gain[None],
        key_gain[None],
        inverse,
        out_weight,
        residual_in,
        norm_gain[None],
        gate_weight,
        up_weight,
        down_weight,
    )


def solution(mesh):
    placed = (
        P(("grp", "sp"), "tp"),
        P(("grp", "sp"), None),
        P(("grp", "sp"), None),
        P(),
        P(),
        P(),
        P(("grp", "sp", "tp"), None),
        P(),
        P("sp", "tp"),
        P("sp", "tp"),
        P("tp", "sp"),
    )
    return jax.shard_map(
        functools.partial(local, mesh.shape["sp"], mesh.shape["tp"]),
        mesh=mesh,
        in_specs=placed,
        out_specs=P(("grp", "sp", "tp"), None),
        check_vma=False,
    )
```

time: 415 us -> 177 us (0.43)
  waiting for transfers between devices: 194 us -> 0 us
  Pallas kernels: 0 us -> 167 us
  matrix products: 105 us -> 0 us
  other arithmetic: 60.3 us -> 0.01 us
  local copies, waits for them, and re-layouts: 27.6 us -> 5.99 us
  between operations: 13.5 us -> 0.02 us
  blocking collectives: 11.4 us -> 0 us
    pallas_call x0 -> x1, Pallas kernels: none -> 167 us  [local(): pl.pallas_call(functools.partial(layer_kernel, n, n_tp), out_shape=jax.Sh...]
    all_gather x3 -> x0, waiting for transfers between devices: 152 us -> none  [the longest x1 117 us: sent_together(): lax.all_gather(both, axis, axis=dim, tiled=True)]
    dot_general x35 -> x0, matrix products: 105 us -> none  [the longest x16 57.4 us: attend_block(): lax.dot_general(query_rot, key_part, (((1,), (1,)), ((), ())), preferred_...]
    reduce_sum x18 -> x0, other arithmetic: 51.8 us -> none  [the longest x16 49.4 us: attend_block(): denominator = denominator * factor + jnp.sum(raised, axis=1)]
    reduce_scatter x1 -> x0, waiting for transfers between devices: 41.5 us -> none  [local(): lax.psum_scatter(jnp.dot(hidden, full_down, preferred_element_type=jnp.fl...]
    all_to_all x1 -> x0, blocking collectives: 11.4 us -> none  [local(): lax.all_to_all(attended, 'tp', split_axis=0, concat_axis=1, tiled=True)]
    unnamed x16 -> x3, local copies, waits for them, and re-layouts: 13.1 us -> 5.15 us
    while x48 -> x0, local copies, waits for them, and re-layouts: 5.87 us -> none
  transfers between devices with their start and end apart: 4 -> 0, of which waited for: 3 -> 0; matrix products, arithmetic and copies ran while one was open for 39% -> 0% of each run, Pallas kernels for 0% -> 0%
where the time goes in v1:
time: 177 us; the launch traced here: 173 us
  Pallas kernels  167 us (94%)
  local copies, waits for them, and re-layouts  5.99 us (3%)
    pallas_call x1, Pallas kernels, local(): pl.pallas_call(functools.partial(layer_kernel, n, n_tp), out_shape=jax.Sh...  167 us
    unnamed x3, local copies, waits for them, and re-layouts  5.15 us

profile of v1, /device:TPU:33, one launch (start us, length us, event | category | flops | bytes accessed | tf_op | source)
XLA Modules:
  0.0 173.4 jit_solution(16742187648581301258)
XLA Ops:
  0.0 0.1 broadcast_in_dim.14
  0.1 0.1 tile.7
  0.2 0.7 broadcast_in_dim_tile.3.inv_ref
  0.9 1.6 copy.14.gate_ref
  2.5 1.6 copy.15.up_ref
  4.1 167.4 %layer.1 = bf16[128,2048]{1,0:T(8,128)(2,1)} custom-call(bf16[1024,128]{1,0:T(8,128)(2,1)} %q_ref.1, bf16[1024,256]{1,0:T(8,128)(2,1)} %k_ref.1, bf16[1024,256]{1,0:T(8,128)(2,1)} %v_ref.1, f32[1,128]{1,0:T(1,128)} %bitcast.4, f32[1,128]{1,0:T(1,128)} %bitcast.5, f32[1,128]{1,0:T(1,128)} %broadcast_in_dim_tile.3.inv_ref, bf16[1024,2048]{1,0:T(8,128)(2,1)} %ow_hbm.1, ...), custom_call_target="tpu_custom_call" | custom-call | tf_op jit(solution)/shard_map/layer/pallas_call | solution.py:674
  171.6 1.9 %copy.17 = bf16[128,2048]{1,0:T(8,128)(2,1)} copy(bf16[128,2048]{1,0:T(8,128)(2,1)} %layer.1) | data formatting | bytes 1048576
  (2 shorter events, 0.0 us)

commit v2 on v1

v2 whole, which is shorter than its diff:
```python
import functools
import math

import jax
import jax.numpy as jnp
import numpy as np
from jax import lax
from jax.experimental import pallas as pl
from jax.experimental.pallas import tpu as pltpu
from jax.sharding import PartitionSpec as P

HQ = 8
KV = 2
HD = 128
GRID_W = 64
MESH = pl.DeviceIdType.MESH
F32 = jnp.float32
BF16 = jnp.bfloat16
ROWS_ATT = 256
ROWS_FF = 256
TILES = 4


def scoped(name):
    def wrapped(f):
        def call(*args):
            with jax.named_scope(name):
                return f(*args)

        return call

    return wrapped


def layer_kernel(
    n,
    n_tp,
    q_ref,
    k_ref,
    v_ref,
    qg_ref,
    kg_ref,
    inv_ref,
    ow_hbm,
    res_ref,
    ng_ref,
    gate_ref,
    up_ref,
    down_ref,
    out_ref,
    kv,
    qrot,
    acc,
    mx,
    ls,
    sa,
    sb,
    ta,
    tb,
    cosr,
    sinr,
    gu,
    dw,
    ow,
    res,
    att,
    nrm,
    mid,
    hid,
    part,
    kept,
    d2s,
    d2r,
    s1s,
    s1r,
    s2s,
    s2r,
    yk,
    zk,
    ow_sem,
    kv_ss,
    kv_rs,
    kx_ss,
    kx_rs,
    kd_ss,
    kd_rs,
    w_ss,
    w_rs,
    y_ss,
    y_rs,
    a_ss,
    a_rs,
    r_ss,
    r_rs,
    t_ss,
    t_rs,
):
    me = lax.axis_index("sp")
    tp = lax.axis_index("tp")
    grp = lax.axis_index("grp")
    odd = lax.rem(grp, 2)
    core = lax.rem(tp, 2)
    x = tp // 2
    tok = q_ref.shape[0]
    d = res_ref.shape[1]
    own_rows = res_ref.shape[0]
    half_n = n // 2
    kv_head = tp // (n_tp // KV)

    def wrap(i):
        return lax.rem(i + n, n)

    right = wrap(me + 1)
    left = wrap(me - 1)
    n1x = x + 1 - 2 * lax.rem(x, 2)
    n2x = 3 - x
    dgx = 3 - n1x
    mate = x * 2 + 1 - core
    n1 = n1x * 2 + core
    n2 = n2x * 2 + core
    dg = dgx * 2 + core
    to_right, to_left = {"sp": right}, {"sp": left}
    to_mate, to_n1, to_n2 = {"tp": mate}, {"tp": n1}, {"tp": n2}
    to_twin = {"grp": grp + 1 - 2 * odd}

    def remote(src, dst, ss, rs, dev):
        return pltpu.make_async_remote_copy(
            src_ref=src, dst_ref=dst, send_sem=ss, recv_sem=rs, device_id=dev, device_id_type=MESH
        )

    load_ow = pltpu.make_async_copy(ow_hbm, ow, ow_sem)
    load_ow.start()

    barrier = pltpu.get_barrier_semaphore()
    for dev in (to_right, to_left, to_mate, to_n1, to_n2, to_twin):
        pl.semaphore_signal(barrier, inc=1, device_id=dev, device_id_type=MESH)

    grid_rows = tok // GRID_W
    lane = lax.broadcasted_iota(jnp.int32, (GRID_W, HD), 1)
    row_pos = (me * grid_rows + lax.broadcasted_iota(jnp.int32, (grid_rows, HD), 0)).astype(F32)
    row_ang = row_pos * inv_ref[...]
    cosr[...] = jnp.cos(row_ang)
    sinr[...] = jnp.sin(row_ang)
    col_ang = lax.broadcasted_iota(jnp.int32, (GRID_W, HD), 0).astype(F32) * inv_ref[...]
    cos_col = jnp.cos(col_ang)
    sin_col = jnp.sin(col_ang)
    even = lax.rem(lane, 2) == 0
    by_row = lane < HD // 2

    def turned(source, gain, i):
        v = source.astype(F32)
        v = v * lax.rsqrt(jnp.mean(v * v, axis=-1, keepdims=True) + 1e-06) * gain
        cosine = jnp.where(by_row, cosr[pl.ds(i, 1), :], cos_col)
        sine = jnp.where(by_row, sinr[pl.ds(i, 1), :], sin_col)
        swapped = jnp.where(even, pltpu.roll(v, HD - 1, 1), pltpu.roll(v, 1, 1))
        signed = jnp.where(even, -sine, sine)
        return (v * cosine + swapped * signed).astype(BF16)

    kv_lanes = pl.ds(pl.multiple_of(kv_head * HD, HD), HD)

    def prep_k(o, _):
        for u in range(TILES):
            i = o * TILES + u
            rows = pl.ds(pl.multiple_of(i * GRID_W, GRID_W), GRID_W)
            kv[me, rows, 0:HD] = turned(k_ref[rows, kv_lanes], kg_ref[...], i)
            kv[me, rows, HD : 2 * HD] = v_ref[rows, kv_lanes]
        return 0

    with jax.named_scope("prepk"):
        lax.fori_loop(0, grid_rows // TILES, prep_k, 0)
        res[pl.ds(pl.multiple_of(tp * own_rows, own_rows), own_rows), :] = res_ref[...]
    with jax.named_scope("barrier"):
        pl.semaphore_wait(barrier, 6)

    quarter = tok // 4
    slab = tok // 2

    side = lax.rem(x, 2)
    share = quarter * 5 // 16
    sizes = (share, share, quarter - 2 * share)

    def block_at(direction, t):
        return wrap(me - t) if direction == 0 else wrap(me + t)

    def piece(direction, t, a, c, which):
        start = (side * share, (1 - side) * share, 2 * share)[which]
        at = pl.multiple_of((2 * a + c) * quarter + start, 16)
        return kv.at[block_at(direction, t), pl.ds(at, sizes[which]), :]

    def kv_ring(direction, t, a, which, late):
        s = piece(direction, t, a, core, which)
        return remote(
            s,
            s,
            kv_ss.at[direction, t, a, which // 2],
            kv_rs.at[direction, t + late, a, which // 2],
            (to_right, to_left)[direction],
        )

    def kv_near(direction, t, a, which):
        s = piece(direction, t, a, core, which)
        return remote(s, s, kx_ss.at[direction, t, a], kx_rs.at[direction, t, a], to_n1)

    def kv_mate(direction, t, a, c, which):
        s = piece(direction, t, a, c, which)
        return remote(
            s, s, kd_ss.at[direction, t, a, which], kd_rs.at[direction, t, a, which], to_mate
        )

    for a in range(2):
        for which in (0, 2):
            for direction in range(2):
                kv_ring(direction, 0, a, which, 1).start()

    strips = 8
    strip = d // strips

    def res_slot(j, h=None):
        rows = pl.ds(pl.multiple_of(j * own_rows, own_rows), own_rows)
        if h is None:
            return res.at[rows, :]
        return res.at[rows, pl.ds(pl.multiple_of(h * strip, strip), strip)]

    def pair(s, ss, rs, i, dev):
        return remote(s, s, ss.at[i], rs.at[i], dev)

    def other(j):
        return j + 1 - 2 * core

    def res_to_n1(j, h):
        return pair(res_slot(j, h), r_ss, r_rs, h, to_n1)

    def res_on(j, h):
        return pair(res_slot(j, h), r_ss, r_rs, strips + h, to_n2)

    def res_to_n2(j):
        return pair(res_slot(j), r_ss, r_rs, 2 * strips, to_n2)

    def res_mate(j, i):
        return pair(res_slot(j), r_ss, r_rs, 2 * strips + 1 + i, to_mate)

    def att_slot(j, i):
        lanes = pl.ds(pl.multiple_of(j * HD, HD), HD)
        return att.at[i * ROWS_ATT : (i + 1) * ROWS_ATT, lanes]

    def att_to(j, i, which):
        return pair(att_slot(j, i), a_ss, a_rs, which * 4 + i, (to_n1, to_n2)[which])

    def att_on(j, i):
        return pair(att_slot(j, i), a_ss, a_rs, 8 + i, to_n2 if i < 2 else to_n1)

    def att_mate(j, i, which):
        return pair(att_slot(j, i), a_ss, a_rs, 12 + which * 4 + i, to_mate)

    def att_send(i):
        att_to(tp, i, 0).start()
        att_to(tp, i, 1).start()
        att_mate(tp, i, 0).start()

    def att_relay(i):
        att_to(n1, i, 0).wait_recv()
        att_to(n2, i, 1).wait_recv()
        att_on(n1 if i < 2 else n2, i).start()
        att_mate(n1, i, 1).start()
        att_mate(n2, i, 2).start()

    def att_diag(i):
        att_on(dg, i).wait_recv()
        att_mate(dg, i, 3).start()

    def att_taken(i):
        for which, j in enumerate((tp, n1, n2, dg)):
            att_mate(other(j), i, which).wait_recv()

    res_to_n2(tp).start()
    res_mate(tp, 0).start()

    gk = gate_ref.shape[1]
    ff = down_ref.shape[0]
    ff_pad = gu.shape[0] // 2

    def w_slot(which, b):
        if which == 2:
            return dw.at[pl.ds(pl.multiple_of(b * ff, ff), ff), :]
        lanes = pl.ds(pl.multiple_of(b * gk, gk), gk)
        row = (odd if which == 0 else 1 - odd) * ff_pad
        return gu.at[pl.ds(pl.multiple_of(row, ff_pad), ff), lanes]

    def w_copy(which, direction, t, late):
        s = w_slot(which, block_at(direction, t))
        return remote(
            s,
            s,
            w_ss.at[which // 2, direction, t],
            w_rs.at[which // 2, direction, t + late],
            (to_right, to_left)[direction],
        )

    def w_twin(which, direction, t):
        s = w_slot(which, block_at(direction, t))
        return remote(s, s, y_ss.at[direction, t], y_rs.at[direction, t], to_twin)

    def w_start(whiches):
        for which in whiches:
            for direction in range(2):
                w_copy(which, direction, 0, 1).start()

    @scoped("wstep")
    def w_step(whiches, t):
        for which in whiches:
            for direction in range(2):
                w_copy(which, direction, t, 0).wait_recv()

                @pl.when((t < half_n - 1) | (core == direction))
                def _():
                    w_copy(which, direction, t, 1).start()

                if which == 0:
                    w_twin(0, direction, t).start()

    @scoped("wlast")
    def w_last():
        for direction in range(2):

            @pl.when(core == direction)
            def _():
                w_copy(0, direction, half_n, 0).wait_recv()
                w_twin(0, direction, half_n).start()
                w_copy(2, direction, half_n, 0).wait_recv()

    @scoped("wtwin")
    def w_taken():
        def one(t, _):
            for direction in range(2):

                @pl.when((t < half_n) | (core == direction))
                def _():
                    w_twin(1, direction, t).wait_recv()

            return 0

        lax.fori_loop(1, half_n + 1, one, 0)

    def w_sent():
        def one(t, _):
            for direction in range(2):

                @pl.when((t < half_n - 1) | (core == direction))
                def _():
                    w_copy(0, direction, t, 1).wait_send()
                    w_copy(2, direction, t, 1).wait_send()

                @pl.when((t < half_n - 1) | (core == direction))
                def _():
                    w_twin(0, direction, t + 1).wait_send()

            return 0

        lax.fori_loop(0, half_n, one, 0)

    def prep_q(o, _):
        for u in range(TILES):
            i = o * TILES + u
            rows = pl.ds(pl.multiple_of(i * GRID_W, GRID_W), GRID_W)
            qrot[rows, :] = turned(q_ref[rows, :], qg_ref[...], i)
        return 0

    with jax.named_scope("prepq"):
        lax.fori_loop(0, grid_rows // TILES, prep_q, 0)
    own_lanes = pl.ds(pl.multiple_of(me * gk, gk), gk)
    gu[0:ff, own_lanes] = gate_ref[...]
    gu[ff_pad : ff_pad + ff, own_lanes] = up_ref[...]
    dw[pl.ds(pl.multiple_of(me * ff, ff), ff), :] = down_ref[...]
    for which in range(2):
        gu[which * ff_pad + ff : (which + 1) * ff_pad, :] = jnp.zeros((ff_pad - ff, gu.shape[1]), BF16)
    mx[...] = jnp.full(mx.shape, -1e30, F32)
    ls[...] = jnp.zeros(ls.shape, F32)
    acc[...] = jnp.zeros(acc.shape, F32)

    factor = HD ** (-0.5) * math.log2(math.e)

    dims = (((1,), (1,)), ((), ()))
    blocks = tok // ROWS_ATT

    def slabs(keys):
        return [(b, pl.ds(pl.multiple_of(h * slab, slab), slab)) for b, h in keys]

    def score(keys, i, s_ref, t_ref):
        q = qrot[i * ROWS_ATT : (i + 1) * ROWS_ATT, :]
        top = None
        for n_slab, (b, r) in enumerate(slabs(keys)):
            s = lax.dot_general(q, kv[b, r, 0:HD], dims, preferred_element_type=F32)
            s_ref[:, n_slab * slab : (n_slab + 1) * slab] = s
            for j in range(slab // HD):
                tile = s[:, j * HD : (j + 1) * HD]
                top = tile if top is None else jnp.maximum(top, tile)
        t_ref[...] = top

    def weigh(keys, i, s_ref, t_ref):
        rows = slice(i * ROWS_ATT, (i + 1) * ROWS_ATT)
        old = mx[rows, :]
        new = jnp.maximum(old, jnp.max(t_ref[...], axis=1, keepdims=True))
        mx[rows, :] = new
        alpha = jnp.exp2((old - new) * factor)
        base = new[:, 0:1]
        total = ls[rows, :] * alpha
        weighted = acc[rows, :] * alpha
        for n_slab, (b, r) in enumerate(slabs(keys)):
            raised = jnp.exp2((s_ref[:, n_slab * slab : (n_slab + 1) * slab] - base) * factor)
            for j in range(slab // HD):
                total = total + raised[:, j * HD : (j + 1) * HD]
            weighted = weighted + jnp.dot(
                raised.astype(BF16), kv[b, r, HD : 2 * HD], preferred_element_type=F32
            )
        ls[rows, :] = total
        acc[rows, :] = weighted

    held = ((sa, ta), (sb, tb))

    def attend_units(units, after=None):
        score(*units[0], *held[0])
        for u, unit in enumerate(units):
            if u + 1 < len(units):
                score(*units[u + 1], *held[(u + 1) % 2])
            weigh(*unit, *held[u % 2])
            if after is not None:
                after(u)

    def keys_of(t, a):
        return ((wrap(me - t), a), (wrap(me + t), a))

    @scoped("attend")
    def attend(keys):
        attend_units([(keys, i) for i in range(blocks)])

    @scoped("take")
    def kv_take(t, a):
        for which in (0, 2):
            for direction in range(2):
                kv_ring(direction, t, a, which, 0).wait_recv()

                @pl.when((t < half_n - 1) | (core == direction))
                def _():
                    kv_ring(direction, t, a, which, 1).start()

                if which == 0:
                    kv_near(direction, t, a, 0).start()
                kv_mate(direction, t, a, core, which).start()

    @scoped("near")
    def near_take(t, a):
        for direction in range(2):
            kv_near(direction, t, a, 1).wait_recv()
            kv_mate(direction, t, a, core, 1).start()

    @scoped("mate")
    def mate_take(t, a):
        for direction in range(2):
            for which in range(3):
                kv_mate(direction, t, a, 1 - core, which).wait_recv()

    def on_last(who, f):
        for direction in range(2):

            @pl.when(who == direction)
            def _():
                for a in range(2):
                    f(direction, a)

    attend(((me, 0), (me, 1)))
    kv_take(1, 0)
    kv_take(1, 1)
    w_start((0, 2))
    kv_take(2, 0)
    near_take(1, 0)

    def phase(p, _):
        kv_take((p + 1) // 2, lax.rem(p + 1, 2))

        @pl.when(p < 4 + strips)
        def _():
            res_to_n1(tp, p - 4).start()

        @pl.when(p >= 15 - strips)
        def _():
            res_to_n1(n1, p - 15 + strips).wait_recv()
            res_on(n1, p - 15 + strips).start()

        @pl.when(lax.rem(p, 3) == 1)
        def _():
            w_step((0,), p // 3)

        @pl.when(lax.rem(p, 3) == 2)
        def _():
            w_step((2,), p // 3)

        @pl.when(p == half_n)
        def _():
            res_to_n2(n2).wait_recv()
            res_mate(n2, 1).start()

        near_take((p - 1) // 2, lax.rem(p - 1, 2))
        tb, ab = (p - 2) // 2, lax.rem(p, 2)
        mate_take(tb, ab)
        attend(keys_of(tb, ab))
        return 0

    lax.fori_loop(4, 2 * half_n - 1, phase, 0)

    def last_take(direction, a):
        for which in (0, 2):
            kv_ring(direction, half_n, a, which, 0).wait_recv()
            if which == 0:
                kv_near(direction, half_n, a, 0).start()
            kv_mate(direction, half_n, a, core, which).start()

    def last_near(direction, a):
        kv_near(direction, half_n, a, 1).wait_recv()
        kv_mate(direction, half_n, a, core, 1).start()

    def last_mate(direction, a):
        for which in range(3):
            kv_mate(direction, half_n, a, 1 - core, which).wait_recv()

    with jax.named_scope("lasttake"):
        on_last(core, last_take)
    near_take(half_n - 1, 0)
    mate_take(half_n - 2, 1)
    attend(keys_of(half_n - 2, 1))
    near_take(half_n - 1, 1)
    w_step((0, 2), 5)
    mate_take(half_n - 1, 0)
    attend(keys_of(half_n - 1, 0))
    with jax.named_scope("lastnear"):
        on_last(core, last_near)
    mate_take(half_n - 1, 1)
    res_mate(n1, 2).start()
    with jax.named_scope("lastmate"):
        on_last(1 - core, last_mate)

    def finish(u):
        if u % 2 == 0:
            return
        i = u // 2
        rows = slice(i * ROWS_ATT, (i + 1) * ROWS_ATT)
        below = jnp.sum(ls[rows, :], axis=1, keepdims=True)
        att[rows, pl.ds(pl.multiple_of(tp * HD, HD), HD)] = (acc[rows, :] / below).astype(BF16)
        if i > 0:
            att_send(i - 1)
        if i == 1:
            w_step((0, 2), 6)

    last_keys = (keys_of(half_n - 1, 1), ((wrap(me + half_n), 0), (wrap(me + half_n), 1)))
    with jax.named_scope("lastattend"):
        attend_units([(last_keys[u % 2], u // 2) for u in range(2 * blocks)], finish)
    att_send(blocks - 1)
    load_ow.wait()
    with jax.named_scope("relay"):
        for i in range(blocks):
            att_relay(i)
    w_step((0, 2), 7)
    with jax.named_scope("diag"):
        for i in range(blocks):
            att_diag(i)
    with jax.named_scope("taken"):
        for i in range(blocks):
            att_taken(i)
        res_mate(other(tp), 0).wait_recv()
        res_mate(other(n2), 1).wait_recv()

    def project(o, _):
        i = jnp.where(o == 0, x, jnp.where(o == 1, n2x, jnp.where(o == 2, n1x, dgx)))

        @pl.when(o == 1)
        def _():
            for h in range(strips):
                res_on(dg, h).wait_recv()
            res_mate(dg, 3).start()
            w_last()

        @pl.when(o == 2)
        def _():
            res_mate(other(n1), 2).wait_recv()

        @pl.when(o == 3)
        def _():
            res_mate(other(dg), 3).wait_recv()

        rows = pl.ds(pl.multiple_of(i * ROWS_FF, ROWS_FF), ROWS_FF)
        middle = res[rows, :].astype(F32) + jnp.dot(
            att[rows, :], ow[...], preferred_element_type=F32
        )
        scale = lax.rsqrt(jnp.mean(middle * middle, axis=-1, keepdims=True) + 1e-06)
        nrm[rows, :] = (middle * scale * ng_ref[...]).astype(BF16)
        for j in range(2):

            @pl.when((o == 0) & (core == j))
            def _():
                mid[...] = middle[j * own_rows : (j + 1) * own_rows, :]

        return 0

    with jax.named_scope("project"):
        lax.fori_loop(0, tok // ROWS_FF, project, 0)
    w_taken()

    def units(i, _):
        rows = pl.ds(pl.multiple_of(i * ROWS_FF, ROWS_FF), ROWS_FF)
        n_rows = nrm[rows, :]
        act = lax.dot_general(n_rows, gu[...], dims, preferred_element_type=F32)
        gate = act[:, 0:ff]
        hid[rows, :] = (gate / (1.0 + jnp.exp(-gate)) * act[:, ff_pad : ff_pad + ff]).astype(BF16)

        return 0

    with jax.named_scope("units"):
        lax.fori_loop(0, tok // ROWS_FF, units, 0)

    near = (n1x, n2x)
    far = (n2x, n1x)
    to_near = (to_n1, to_n2)
    to_far = (to_n2, to_n1)

    def col_block(g, k):
        return wrap(me - k) if g == 0 else wrap(me + k + 1)

    def d2_copy(g, k):
        return remote(d2s.at[g, k], d2r.at[g, k], t_ss.at[0, g, k], t_rs.at[0, g, k], to_mate)

    def s1_copy(g, k):
        return remote(s1s.at[g, k], s1r.at[g, k], t_ss.at[1, g, k], t_rs.at[1, g, k], to_near[g])

    def s2_copy(g, k):
        return remote(s2s.at[g, k], s2r.at[g, k], t_ss.at[2, g, k], t_rs.at[2, g, k], to_far[g])

    @scoped("stage0")
    def stage0(k):
        for g in range(2):
            b = col_block(g, k)
            part[...] = jnp.dot(
                hid[...],
                dw[pl.ds(pl.multiple_of(b * ff, ff), ff), :],
                preferred_element_type=F32,
            )
            for c in range(4):
                rows = slice(c * own_rows, (c + 1) * own_rows)
                theirs = pl.ds(pl.multiple_of((c * 2 + 1 - core) * own_rows, own_rows), own_rows)
                mine = pl.ds(pl.multiple_of((c * 2 + core) * own_rows, own_rows), own_rows)
                d2s[g, k, rows, :] = part[theirs, :].astype(BF16)
                kept[g, k, rows, :] = part[mine, :]
            d2_copy(g, k).start()

    @scoped("stage1")
    def stage1(k):
        for g in range(2):
            d2_copy(g, k).wait_recv()

            def summed(c):
                at = pl.ds(pl.multiple_of(c * own_rows, own_rows), own_rows)
                return kept[g, k, at, :] + d2r[g, k, at, :].astype(F32)

            s1s[g, k, 0:own_rows, :] = summed(near[g]).astype(BF16)
            s1s[g, k, own_rows : 2 * own_rows, :] = summed(dgx).astype(BF16)
            yk[g, k, 0] = summed(x)
            yk[g, k, 1] = summed(far[g])
            s1_copy(g, k).start()

    @scoped("stage2")
    def stage2(k):
        for g in range(2):
            s1_copy(g, k).wait_recv()
            s2s[g, k] = (
                yk[g, k, 1] + s1r[g, k, own_rows : 2 * own_rows, :].astype(F32)
            ).astype(BF16)
            zk[g, k] = yk[g, k, 0] + s1r[g, k, 0:own_rows, :].astype(F32)
            s2_copy(g, k).start()

    @scoped("stage3")
    def stage3(k):
        for g in range(2):
            s2_copy(g, k).wait_recv()
            lanes = pl.ds(pl.multiple_of(col_block(g, k) * HD, HD), HD)
            out_ref[:, lanes] = (mid[:, lanes] + zk[g, k] + s2r[g, k].astype(F32)).astype(BF16)

    lag = 2

    def columns(k, _):
        @pl.when(k < half_n)
        def _():
            stage0(k)

        @pl.when(k >= lag)
        def _():
            stage1(k - lag)

        return 0

    lax.fori_loop(0, half_n + lag, columns, 0)

    def sums(k, _):
        @pl.when(k < half_n)
        def _():
            stage2(k)

        @pl.when(k >= lag)
        def _():
            stage3(k - lag)

        return 0

    lax.fori_loop(0, half_n + lag, sums, 0)

    def kv_sent(t, _):
        for a in range(2):
            for direction in range(2):
                for which in (0, 2):

                    @pl.when((t < half_n - 1) | (core == direction))
                    def _():
                        kv_ring(direction, t, a, which, 1).wait_send()

                @pl.when(t > 0)
                def _():
                    kv_near(direction, t, a, 0).wait_send()
                    for which in range(3):
                        kv_mate(direction, t, a, core, which).wait_send()

        return 0

    lax.fori_loop(0, half_n, kv_sent, 0)

    def last_sent(direction, a):
        kv_near(direction, half_n, a, 0).wait_send()
        for which in range(3):
            kv_mate(direction, half_n, a, core, which).wait_send()

    on_last(core, last_sent)
    w_sent()
    for h in range(strips):
        res_to_n1(tp, h).wait_send()
        res_on(n1, h).wait_send()
    res_to_n2(tp).wait_send()
    for i, j in enumerate((tp, n2, n1, dg)):
        res_mate(j, i).wait_send()
    for i in range(blocks):
        att_to(tp, i, 0).wait_send()
        att_to(tp, i, 1).wait_send()
        att_on(n1 if i < 2 else n2, i).wait_send()
        for which, j in enumerate((tp, n1, n2, dg)):
            att_mate(j, i, which).wait_send()

    def sums_sent(k, _):
        for g in range(2):
            d2_copy(g, k).wait_send()
            s1_copy(g, k).wait_send()
            s2_copy(g, k).wait_send()
        return 0

    lax.fori_loop(0, half_n, sums_sent, 0)


def local(
    n,
    n_tp,
    queries,
    keys,
    values,
    query_gain,
    key_gain,
    out_weight,
    residual_in,
    norm_gain,
    gate_weight,
    up_weight,
    down_weight,
):
    tok = queries.shape[0]
    own_rows, d = residual_in.shape
    ff = down_weight.shape[0]
    gk = gate_weight.shape[0]
    ff_pad = -(-ff // HD) * HD
    half = HD // 2
    half_n = n // 2
    inverse = 10000.0 ** (-np.arange(0, half, 2, dtype=np.float32) / half)
    inverse = jnp.asarray(np.tile(np.repeat(inverse, 2), 2)[None].astype(np.float32))
    vmem = pl.BlockSpec(memory_space=pltpu.VMEM)
    dma = pltpu.SemaphoreType.DMA
    scratch = [
        pltpu.VMEM((n, tok, 2 * HD), BF16),
        pltpu.VMEM((tok, HD), BF16),
        pltpu.VMEM((tok, HD), F32),
        pltpu.VMEM((tok, HD), F32),
        pltpu.VMEM((tok, HD), F32),
        pltpu.VMEM((ROWS_ATT, tok), F32),
        pltpu.VMEM((ROWS_ATT, tok), F32),
        pltpu.VMEM((ROWS_ATT, HD), F32),
        pltpu.VMEM((ROWS_ATT, HD), F32),
        pltpu.VMEM((tok // GRID_W, HD), F32),
        pltpu.VMEM((tok // GRID_W, HD), F32),
        pltpu.VMEM((2 * ff_pad, n * gk), BF16),
        pltpu.VMEM((n * ff, HD), BF16),
        pltpu.VMEM(out_weight.shape, BF16),
        pltpu.VMEM((tok, d), BF16),
        pltpu.VMEM((tok, HQ * HD), BF16),
        pltpu.VMEM((tok, d), BF16),
        pltpu.VMEM((own_rows, d), F32),
        pltpu.VMEM((tok, ff), BF16),
        pltpu.VMEM((tok, HD), F32),
        pltpu.VMEM((2, half_n, tok // 2, HD), F32),
        pltpu.VMEM((2, half_n, tok // 2, HD), BF16),
        pltpu.VMEM((2, half_n, tok // 2, HD), BF16),
        pltpu.VMEM((2, half_n, 2 * own_rows, HD), BF16),
        pltpu.VMEM((2, half_n, 2 * own_rows, HD), BF16),
        pltpu.VMEM((2, half_n, own_rows, HD), BF16),
        pltpu.VMEM((2, half_n, own_rows, HD), BF16),
        pltpu.VMEM((2, half_n, 2, own_rows, HD), F32),
        pltpu.VMEM((2, half_n, own_rows, HD), F32),
        dma,
        dma((2, half_n + 1, 2, 2)),
        dma((2, half_n + 1, 2, 2)),
        dma((2, half_n + 1, 2)),
        dma((2, half_n + 1, 2)),
        dma((2, half_n + 1, 2, 3)),
        dma((2, half_n + 1, 2, 3)),
        dma((2, 2, half_n + 1)),
        dma((2, 2, half_n + 1)),
        dma((2, half_n + 1)),
        dma((2, half_n + 1)),
        dma((28,)),
        dma((28,)),
        dma((21,)),
        dma((21,)),
        dma((3, 2, half_n)),
        dma((3, 2, half_n)),
    ]
    specs = [vmem] * 12
    specs[6] = pl.BlockSpec(memory_space=pl.ANY)
    return pl.pallas_call(
        functools.partial(layer_kernel, n, n_tp),
        out_shape=jax.ShapeDtypeStruct((own_rows, d), BF16),
        in_specs=specs,
        out_specs=vmem,
        scratch_shapes=scratch,
        compiler_params=pltpu.CompilerParams(
            collective_id=0, has_side_effects=True, vmem_limit_bytes=67043328
        ),
        name="layer",
    )(
        queries,
        keys,
        values,
        query_gain[None],
        key_gain[None],
        inverse,
        out_weight,
        residual_in,
        norm_gain[None],
        gate_weight.T,
        up_weight.T,
        down_weight,
    )


def solution(mesh):
    placed = (
        P(("grp", "sp"), "tp"),
        P(("grp", "sp"), None),
        P(("grp", "sp"), None),
        P(),
        P(),
        P(),
        P(("grp", "sp", "tp"), None),
        P(),
        P("sp", "tp"),
        P("sp", "tp"),
        P("tp", "sp"),
    )
    return jax.shard_map(
        functools.partial(local, mesh.shape["sp"], mesh.shape["tp"]),
        mesh=mesh,
        in_specs=placed,
        out_specs=P(("grp", "sp", "tp"), None),
        check_vma=False,
    )
```

time: 177 us -> 140 us (0.79); the launches traced: 173 us -> 139 us
  Pallas kernels: 167 us -> 137 us
  local copies, waits for them, and re-layouts: 5.99 us -> 1.88 us
    pallas_call x1, Pallas kernels: 167 us -> 137 us  [local(): pl.pallas_call(functools.partial(layer_kernel, n, n_tp), out_shape=jax.Sh...]
    unnamed x3 -> x1, local copies, waits for them, and re-layouts: 5.15 us -> 1.88 us
where the time goes in v2:
time: 140 us; the launch traced here: 139 us
  Pallas kernels  137 us (98%)
  local copies, waits for them, and re-layouts  1.88 us (1%)
    pallas_call x1, Pallas kernels, local(): pl.pallas_call(functools.partial(layer_kernel, n, n_tp), out_shape=jax.Sh...  137 us

profile of v2, /device:TPU:33, one launch (start us, length us, event | category | flops | bytes accessed | tf_op | source)
XLA Modules:
  0.0 139.2 jit_solution(17110561452791177070)
XLA Ops:
  0.0 137.3 %layer.1 = bf16[128,2048]{1,0:T(8,128)(2,1)} custom-call(bf16[1024,128]{1,0:T(8,128)(2,1)} %q_ref.1, bf16[1024,256]{1,0:T(8,128)(2,1)} %k_ref.1, bf16[1024,256]{1,0:T(8,128)(2,1)} %v_ref.1, f32[1,128]{1,0:T(1,128)} %bitcast.8, f32[1,128]{1,0:T(1,128)} %bitcast.9, f32[1,128]{1,0:T(1,128)} %constant.2.clone.inv_ref, bf16[1024,2048]{1,0:T(8,128)(2,1)} %ow_hbm.1, ...), custom_call_target="tpu_custom_call" | custom-call | tf_op jit(solution)/shard_map/layer/pallas_call | solution.py:838
  137.3 1.9 %copy.14 = bf16[128,2048]{1,0:T(8,128)(2,1)} copy(bf16[128,2048]{1,0:T(8,128)(2,1)} %layer.1) | data formatting | bytes 1048576

commit v3 on v2

v3 whole, which is shorter than its diff:
```python
import functools
import math

import jax
import jax.numpy as jnp
import numpy as np
from jax import lax
from jax.experimental import pallas as pl
from jax.experimental.pallas import tpu as pltpu
from jax.sharding import PartitionSpec as P

HQ = 8
KV = 2
HD = 128
GRID_W = 64
MESH = pl.DeviceIdType.MESH
F32 = jnp.float32
BF16 = jnp.bfloat16
ROWS_ATT = 256
ROWS_FF = 256
TILES = 4


def scoped(name):
    def wrapped(f):
        def call(*args):
            with jax.named_scope(name):
                return f(*args)

        return call

    return wrapped


def layer_kernel(
    n,
    n_tp,
    q_ref,
    k_ref,
    v_ref,
    qg_ref,
    kg_ref,
    inv_ref,
    ow_hbm,
    res_ref,
    ng_ref,
    gate_ref,
    up_ref,
    down_ref,
    out_ref,
    kv,
    qrot,
    acc,
    mx,
    ls,
    sa,
    sb,
    ta,
    tb,
    cosr,
    sinr,
    gu,
    dw,
    ow,
    res,
    att,
    nrm,
    mid,
    hid,
    part,
    d2s,
    d2r,
    yk,
    xs,
    xr,
    ow_sem,
    kv_ss,
    kv_rs,
    kx_rs,
    kd_rs,
    w_ss,
    w_rs,
    y_rs,
    a_ss,
    a_rs,
    r_ss,
    r_rs,
    t_ss,
    t_rs,
):
    me = lax.axis_index("sp")
    tp = lax.axis_index("tp")
    grp = lax.axis_index("grp")
    odd = lax.rem(grp, 2)
    core = lax.rem(tp, 2)
    x = tp // 2
    tok = q_ref.shape[0]
    d = res_ref.shape[1]
    own_rows = res_ref.shape[0]
    half_n = n // 2
    kv_head = tp // (n_tp // KV)

    def wrap(i):
        return lax.rem(i + n, n)

    right = wrap(me + 1)
    left = wrap(me - 1)
    n1x = x + 1 - 2 * lax.rem(x, 2)
    n2x = 3 - x
    dgx = 3 - n1x
    mate = x * 2 + 1 - core
    n1 = n1x * 2 + core
    n2 = n2x * 2 + core
    dg = dgx * 2 + core
    to_right, to_left = {"sp": right}, {"sp": left}
    to_mate, to_n1, to_n2 = {"tp": mate}, {"tp": n1}, {"tp": n2}
    to_twin = {"grp": grp + 1 - 2 * odd}

    def remote(src, dst, ss, rs, dev):
        return pltpu.make_async_remote_copy(
            src_ref=src, dst_ref=dst, send_sem=ss, recv_sem=rs, device_id=dev, device_id_type=MESH
        )

    def arrived(span, sem):
        pltpu.make_async_copy(span, span, sem).wait()

    load_ow = pltpu.make_async_copy(ow_hbm, ow, ow_sem)
    load_ow.start()

    barrier = pltpu.get_barrier_semaphore()
    for dev in (to_right, to_left, to_mate, to_n1, to_n2, to_twin):
        pl.semaphore_signal(barrier, inc=1, device_id=dev, device_id_type=MESH)

    grid_rows = tok // GRID_W
    lane = lax.broadcasted_iota(jnp.int32, (GRID_W, HD), 1)
    row_pos = (me * grid_rows + lax.broadcasted_iota(jnp.int32, (grid_rows, HD), 0)).astype(F32)
    row_ang = row_pos * inv_ref[...]
    cosr[...] = jnp.cos(row_ang)
    sinr[...] = jnp.sin(row_ang)
    col_ang = lax.broadcasted_iota(jnp.int32, (GRID_W, HD), 0).astype(F32) * inv_ref[...]
    cos_col = jnp.cos(col_ang)
    sin_col = jnp.sin(col_ang)
    even = lax.rem(lane, 2) == 0
    by_row = lane < HD // 2

    def turned(source, gain, i):
        v = source.astype(F32)
        v = v * lax.rsqrt(jnp.mean(v * v, axis=-1, keepdims=True) + 1e-06) * gain
        cosine = jnp.where(by_row, cosr[pl.ds(i, 1), :], cos_col)
        sine = jnp.where(by_row, sinr[pl.ds(i, 1), :], sin_col)
        swapped = jnp.where(even, pltpu.roll(v, HD - 1, 1), pltpu.roll(v, 1, 1))
        signed = jnp.where(even, -sine, sine)
        return (v * cosine + swapped * signed).astype(BF16)

    kv_lanes = pl.ds(pl.multiple_of(kv_head * HD, HD), HD)

    def prep_k(o, _):
        for u in range(TILES):
            i = o * TILES + u
            rows = pl.ds(pl.multiple_of(i * GRID_W, GRID_W), GRID_W)
            kv[me, rows, 0:HD] = turned(k_ref[rows, kv_lanes], kg_ref[...], i)
            kv[me, rows, HD : 2 * HD] = v_ref[rows, kv_lanes]
        return 0

    with jax.named_scope("prepk"):
        lax.fori_loop(0, grid_rows // TILES, prep_k, 0)
        res[pl.ds(pl.multiple_of(tp * own_rows, own_rows), own_rows), :] = res_ref[...]
    with jax.named_scope("barrier"):
        pl.semaphore_wait(barrier, 6)

    quarter = tok // 4
    slab = tok // 2

    side = lax.rem(x, 2)
    share = quarter * 5 // 16
    sizes = (share, share, quarter - 2 * share)

    def block_at(direction, t):
        return wrap(me - t) if direction == 0 else wrap(me + t)

    def piece(direction, t, a, c, which):
        start = (side * share, (1 - side) * share, 2 * share)[which]
        at = pl.multiple_of((2 * a + c) * quarter + start, 16)
        return kv.at[block_at(direction, t), pl.ds(at, sizes[which]), :]

    def kv_ring(direction, t, a, which, late):
        s = piece(direction, t, a, core, which)
        return remote(
            s,
            s,
            kv_ss.at[t],
            kv_rs.at[t + late, a, which // 2],
            (to_right, to_left)[direction],
        )

    def kv_near(direction, t, a, which):
        s = piece(direction, t, a, core, which)
        return remote(s, s, kv_ss.at[t], kx_rs.at[t, a], to_n1)

    def kv_mate(direction, t, a, c, which):
        s = piece(direction, t, a, c, which)
        return remote(s, s, kv_ss.at[t], kd_rs.at[t, a], to_mate)

    def kv_span(rows):
        return kv.at[0, 0:rows]

    for a in range(2):
        for which in (0, 2):
            for direction in range(2):
                kv_ring(direction, 0, a, which, 1).start()

    strips = 8
    strip = d // strips

    def res_slot(j, h=None):
        rows = pl.ds(pl.multiple_of(j * own_rows, own_rows), own_rows)
        if h is None:
            return res.at[rows, :]
        return res.at[rows, pl.ds(pl.multiple_of(h * strip, strip), strip)]

    def pair(s, ss, rs, i, dev):
        return remote(s, s, ss, rs.at[i], dev)

    def other(j):
        return j + 1 - 2 * core

    def res_to_n1(j, h):
        return pair(res_slot(j, h), r_ss, r_rs, h, to_n1)

    def res_on(j, h):
        return pair(res_slot(j, h), r_ss, r_rs, strips, to_n2)

    def res_to_n2(j):
        return pair(res_slot(j), r_ss, r_rs, strips + 1, to_n2)

    def res_mate(j, i):
        return pair(res_slot(j), r_ss, r_rs, strips + 2, to_mate)

    def att_slot(j, i):
        lanes = pl.ds(pl.multiple_of(j * HD, HD), HD)
        return att.at[i * ROWS_ATT : (i + 1) * ROWS_ATT, lanes]

    def att_to(j, i, which):
        return pair(att_slot(j, i), a_ss, a_rs, i, (to_n1, to_n2)[which])

    def att_on(j, i):
        return pair(att_slot(j, i), a_ss, a_rs, 4 + i, to_n2 if i < 2 else to_n1)

    def att_mate(j, i, which):
        return pair(att_slot(j, i), a_ss, a_rs, 8 + i, to_mate)

    def att_send(i):
        att_to(tp, i, 0).start()
        att_to(tp, i, 1).start()
        att_mate(tp, i, 0).start()

    def att_relay(i):
        arrived(att.at[0:ROWS_ATT, 0 : 2 * HD], a_rs.at[i])
        att_on(n1 if i < 2 else n2, i).start()
        att_mate(n1, i, 1).start()
        att_mate(n2, i, 2).start()

    def att_diag(i):
        att_on(dg, i).wait_recv()
        att_mate(dg, i, 3).start()

    def att_taken(i):
        arrived(att.at[0:ROWS_ATT, 0 : 4 * HD], a_rs.at[8 + i])

    def res_pass(h):
        res_to_n1(n1, h).wait_recv()
        res_on(n1, h).start()

    res_to_n2(tp).start()
    res_mate(tp, 0).start()

    gk = gate_ref.shape[1]
    ff = down_ref.shape[0]
    ff_pad = gu.shape[0] // 2

    def w_slot(which, b):
        if which == 2:
            return dw.at[:, pl.ds(pl.multiple_of(b * HD, HD), HD)]
        lanes = pl.ds(pl.multiple_of(b * gk, gk), gk)
        row = (odd if which == 0 else 1 - odd) * ff_pad
        return gu.at[pl.ds(pl.multiple_of(row, ff_pad), ff), lanes]

    def w_copy(which, direction, t, late):
        s = w_slot(which, block_at(direction, t))
        return remote(
            s,
            s,
            w_ss.at[which // 2, t],
            w_rs.at[which // 2, t + late],
            (to_right, to_left)[direction],
        )

    def w_twin(which, direction, t):
        s = w_slot(which, block_at(direction, t))
        return remote(s, s, w_ss.at[0, t], y_rs, to_twin)

    def w_span(which, count):
        return (gu, None, dw)[which].at[0:ff, 0 : count * gk]

    def w_start(whiches):
        for which in whiches:
            for direction in range(2):
                w_copy(which, direction, 0, 1).start()

    @scoped("wstep")
    def w_step(whiches, t):
        for which in whiches:
            arrived(w_span(which, 2), w_rs.at[which // 2, t])
            for direction in range(2):

                @pl.when((t < half_n - 1) | (core == direction))
                def _():
                    w_copy(which, direction, t, 1).start()

                if which == 0:
                    w_twin(0, direction, t).start()

    def w_last(which):
        for direction in range(2):

            @pl.when(core == direction)
            def _():
                arrived(w_span(which, 1), w_rs.at[which // 2, half_n])
                if which == 0:
                    w_twin(0, direction, half_n).start()

    w_order = [(2, 2)]
    for t in range(4, half_n + 1):
        w_order += [(0, t), (2, t - 1)]
    w_order += [(2, half_n)]

    @scoped("pump")
    def pump(count=1):
        for _ in range(count):
            which, t = w_order.pop(0)
            if t < half_n:
                w_step((which,), t)
            else:
                w_last(which)

    @scoped("wtwin")
    def w_taken():
        arrived(w_span(0, n - 1), y_rs)

    def w_sent():
        for t in range(half_n + 1):
            ring = 2 if t < half_n - 1 else half_n - t
            twin = 0 if t == 0 else 2 if t < half_n else 1
            arrived(w_span(0, ring + twin), w_ss.at[0, t])
            if ring > 0:
                arrived(w_span(2, ring), w_ss.at[1, t])

    def prep_q(o, _):
        for u in range(TILES):
            i = o * TILES + u
            rows = pl.ds(pl.multiple_of(i * GRID_W, GRID_W), GRID_W)
            qrot[rows, :] = turned(q_ref[rows, :], qg_ref[...], i)
        return 0

    with jax.named_scope("prepq"):
        lax.fori_loop(0, grid_rows // TILES, prep_q, 0)
    own_lanes = pl.ds(pl.multiple_of(me * gk, gk), gk)
    gu[0:ff, own_lanes] = gate_ref[...]
    gu[ff_pad : ff_pad + ff, own_lanes] = up_ref[...]
    dw[:, pl.ds(pl.multiple_of(me * HD, HD), HD)] = down_ref[...]
    for which in range(2):
        gu[which * ff_pad + ff : (which + 1) * ff_pad, :] = jnp.zeros((ff_pad - ff, gu.shape[1]), BF16)
    mx[...] = jnp.full(mx.shape, -1e30, F32)
    ls[...] = jnp.zeros(ls.shape, F32)
    acc[...] = jnp.zeros(acc.shape, F32)

    factor = HD ** (-0.5) * math.log2(math.e)

    dims = (((1,), (1,)), ((), ()))
    blocks = tok // ROWS_ATT

    def slabs(keys):
        return [(b, pl.ds(pl.multiple_of(h * slab, slab), slab)) for b, h in keys]

    def score(keys, i, s_ref, t_ref):
        q = qrot[i * ROWS_ATT : (i + 1) * ROWS_ATT, :]
        top = None
        for n_slab, (b, r) in enumerate(slabs(keys)):
            s = lax.dot_general(q, kv[b, r, 0:HD], dims, preferred_element_type=F32)
            s_ref[:, n_slab * slab : (n_slab + 1) * slab] = s
            for j in range(slab // HD):
                tile = s[:, j * HD : (j + 1) * HD]
                top = tile if top is None else jnp.maximum(top, tile)
        t_ref[...] = top

    def weigh(keys, i, s_ref, t_ref):
        rows = slice(i * ROWS_ATT, (i + 1) * ROWS_ATT)
        old = mx[rows, :]
        new = jnp.maximum(old, jnp.max(t_ref[...], axis=1, keepdims=True))
        mx[rows, :] = new
        alpha = jnp.exp2((old - new) * factor)
        base = new[:, 0:1]
        total = ls[rows, :] * alpha
        weighted = acc[rows, :] * alpha
        for n_slab, (b, r) in enumerate(slabs(keys)):
            raised = jnp.exp2((s_ref[:, n_slab * slab : (n_slab + 1) * slab] - base) * factor)
            for j in range(slab // HD):
                total = total + raised[:, j * HD : (j + 1) * HD]
            weighted = weighted + jnp.dot(
                raised.astype(BF16), kv[b, r, HD : 2 * HD], preferred_element_type=F32
            )
        ls[rows, :] = total
        acc[rows, :] = weighted

    held = ((sa, ta), (sb, tb))

    def attend_units(units, after=None):
        score(*units[0], *held[0])
        for u, unit in enumerate(units):
            if u + 1 < len(units):
                score(*units[u + 1], *held[(u + 1) % 2])
            weigh(*unit, *held[u % 2])
            if after is not None:
                after(u)

    def keys_of(t, a):
        return ((wrap(me - t), a), (wrap(me + t), a))

    @scoped("attend")
    def attend(keys):
        attend_units([(keys, i) for i in range(blocks)])

    @scoped("take")
    def kv_take(t, a):
        for which in (0, 2):
            arrived(kv_span(2 * sizes[which]), kv_rs.at[t, a, which // 2])
            for direction in range(2):

                @pl.when((t < half_n - 1) | (core == direction))
                def _():
                    kv_ring(direction, t, a, which, 1).start()

                if which == 0:
                    kv_near(direction, t, a, 0).start()
                kv_mate(direction, t, a, core, which).start()

    @scoped("near")
    def near_take(t, a):
        arrived(kv_span(2 * share), kx_rs.at[t, a])
        for direction in range(2):
            kv_mate(direction, t, a, core, 1).start()

    @scoped("mate")
    def mate_take(t, a):
        arrived(kv_span(2 * quarter), kd_rs.at[t, a])

    def on_last(who, f):
        for direction in range(2):

            @pl.when(who == direction)
            def _():
                for a in range(2):
                    f(direction, a)

    attend(((me, 0), (me, 1)))
    kv_take(1, 0)
    kv_take(1, 1)
    kv_take(2, 0)
    near_take(1, 0)

    def phase(p, _):
        kv_take((p + 1) // 2, lax.rem(p + 1, 2))

        @pl.when(p < 8)
        def _():
            res_to_n1(tp, p - 4).start()

        @pl.when((lax.rem(p, 2) == 0) & (p >= 8))
        def _():
            res_to_n1(tp, p // 2).start()

        @pl.when(p >= 8)
        def _():
            res_pass(p - 8)

        @pl.when(p == 8)
        def _():
            w_start((0,))

        @pl.when((lax.rem(p, 2) == 0) & (p >= 10))
        def _():
            w_step((0,), (p - 8) // 2)

        @pl.when(p == 9)
        def _():
            w_start((2,))

        @pl.when(p == 13)
        def _():
            w_step((2,), 1)

        @pl.when(p == half_n)
        def _():
            res_to_n2(n2).wait_recv()
            res_mate(n2, 1).start()

        near_take((p - 1) // 2, lax.rem(p - 1, 2))
        tb, ab = (p - 2) // 2, lax.rem(p, 2)
        mate_take(tb, ab)
        attend(keys_of(tb, ab))
        return 0

    lax.fori_loop(4, 2 * half_n - 1, phase, 0)

    def last_take(direction, a):
        for which in (0, 2):
            arrived(kv_span(sizes[which]), kv_rs.at[half_n, a, which // 2])
            if which == 0:
                kv_near(direction, half_n, a, 0).start()
            kv_mate(direction, half_n, a, core, which).start()

    def last_near(direction, a):
        arrived(kv_span(share), kx_rs.at[half_n, a])
        kv_mate(direction, half_n, a, core, 1).start()

    def last_mate(direction, a):
        arrived(kv_span(quarter), kd_rs.at[half_n, a])

    with jax.named_scope("lasttake"):
        on_last(core, last_take)
    near_take(half_n - 1, 0)
    mate_take(half_n - 2, 1)
    near_take(half_n - 1, 1)
    mate_take(half_n - 1, 0)
    pump()
    relay, diag, taken = scoped("relay")(att_relay), scoped("diag")(att_diag), scoped("taken")(att_taken)

    last_keys = (
        keys_of(half_n - 2, 1),
        keys_of(half_n - 1, 0),
        keys_of(half_n - 1, 1),
        ((wrap(me + half_n), 0), (wrap(me + half_n), 1)),
    )
    order = [(0, 0), (1, 0), (2, 0), (0, 1), (3, 0), (1, 1), (2, 1), (3, 1)]
    order += [(g, i) for i in range(2, blocks) for g in range(4)]

    def finish(u):
        if u == 0:
            mate_take(half_n - 1, 1)
        if u == 1:
            with jax.named_scope("lastnear"):
                on_last(core, last_near)
            res_pass(7)
            res_mate(n1, 2).start()
        if u == 2:
            with jax.named_scope("lastmate"):
                on_last(1 - core, last_mate)
        if u > 0 and order[u - 1][0] == 3:
            att_send(order[u - 1][1])
        g, i = order[u]
        if g != 3:
            return
        rows = slice(i * ROWS_ATT, (i + 1) * ROWS_ATT)
        below = jnp.sum(ls[rows, :], axis=1, keepdims=True)
        att[rows, pl.ds(pl.multiple_of(tp * HD, HD), HD)] = (acc[rows, :] / below).astype(BF16)
        pump()
        if i == 2:
            relay(0)

    with jax.named_scope("lastattend"):
        attend_units([(last_keys[g], i) for g, i in order], finish)
    att_send(blocks - 1)
    with jax.named_scope("resdiag"):
        arrived(res.at[0:own_rows], r_rs.at[strips])
        res_mate(dg, 3).start()
    load_ow.wait()

    @scoped("project")
    def project(i):
        rows = slice(i * ROWS_FF, (i + 1) * ROWS_FF)
        middle = res[rows, :].astype(F32) + jnp.dot(
            att[rows, :], ow[...], preferred_element_type=F32
        )
        scale = lax.rsqrt(jnp.mean(middle * middle, axis=-1, keepdims=True) + 1e-06)
        nrm[rows, :] = (middle * scale * ng_ref[...]).astype(BF16)
        for j in range(2):

            @pl.when(tp == 2 * i + j)
            def _():
                mid[...] = middle[j * own_rows : (j + 1) * own_rows, :]

    relay(1)
    pump()
    diag(0)
    relay(2)
    pump()
    with jax.named_scope("resmate"):
        arrived(res.at[0 : 4 * own_rows], r_rs.at[strips + 2])
    taken(0)
    project(0)
    relay(3)
    diag(1)
    pump()
    taken(1)
    project(1)
    diag(2)
    pump()
    taken(2)
    project(2)
    diag(3)
    pump()
    taken(3)
    project(3)
    w_taken()

    half_d = d // 2
    cols = (slice(0, half_d), slice(half_d, d))
    owners = (dgx, n1x, n2x, x)

    def d2_copy(o):
        return remote(d2s.at[o], d2r.at[o], t_ss, t_rs.at[o], to_mate)

    def x_copy(m):
        dev = (to_n1, to_n2, to_n1, to_n1, to_n2, to_n2)[m]
        return remote(xs.at[m], xr.at[m], t_ss, t_rs.at[4 + m], dev)

    @scoped("units")
    def units(o):
        rows = pl.ds(pl.multiple_of(owners[o] * ROWS_FF, ROWS_FF), ROWS_FF)
        act = lax.dot_general(nrm[rows, :], gu[...], dims, preferred_element_type=F32)
        gate = act[:, 0:ff]
        hid[o] = (gate / (1.0 + jnp.exp(-gate)) * act[:, ff_pad : ff_pad + ff]).astype(BF16)

    @scoped("block")
    def block(o):
        part[...] = jnp.dot(hid[o], dw[...], preferred_element_type=F32)
        theirs = pl.ds(pl.multiple_of((1 - core) * own_rows, own_rows), own_rows)
        mine = pl.ds(pl.multiple_of(core * own_rows, own_rows), own_rows)
        d2s[o] = part[theirs, :].astype(BF16)
        yk[o] = part[mine, :]
        d2_copy(o).start()

    def both(o, c):
        return yk[o, :, cols[c]] + d2r[o, :, cols[c]].astype(F32)

    @scoped("sums")
    def sums(o):
        d2_copy(o).wait_recv()
        if o == 0:
            for c in range(2):
                xs[c] = both(0, c).astype(BF16)
                x_copy(c).start()
        elif o == 1:
            xs[2] = both(1, 0).astype(BF16)
            x_copy(2).start()
            yk[1, :, cols[1]] = both(1, 1)
        elif o == 2:
            xs[4] = both(2, 1).astype(BF16)
            x_copy(4).start()
            yk[2, :, cols[0]] = both(2, 0)
        else:
            for c in range(2):
                yk[3, :, cols[c]] = both(3, c) + mid[:, cols[c]]

    units(0)
    pump()
    units(1)
    units(2)
    pump()
    units(3)
    pump(len(w_order))
    block(0)
    sums(0)
    block(1)
    block(2)
    sums(1)
    block(3)
    sums(2)
    sums(3)
    with jax.named_scope("pass"):
        x_copy(1).wait_recv()
        xs[3] = (yk[1, :, cols[1]] + xr[1].astype(F32)).astype(BF16)
        x_copy(3).start()
        x_copy(0).wait_recv()
        xs[5] = (yk[2, :, cols[0]] + xr[0].astype(F32)).astype(BF16)
        x_copy(5).start()
    for t in range(half_n + 1):
        ring = (2 if t < half_n - 1 else half_n - t) * 2 * (quarter - share)
        others = 0 if t == 0 else (2 if t < half_n else 1) * 2 * (share + quarter)
        arrived(kv.at[0:2, 0 : (ring + others) // 2], kv_ss.at[t])
    w_sent()
    arrived(res.at[0 : 7 * own_rows], r_ss)
    arrived(att.at[:, 0 : 7 * HD], a_ss)
    with jax.named_scope("final"):
        for c, (m1, m2) in enumerate(((2, 5), (4, 3))):
            x_copy(m1).wait_recv()
            x_copy(m2).wait_recv()
            out_ref[:, cols[c]] = (
                yk[3, :, cols[c]] + xr[m1].astype(F32) + xr[m2].astype(F32)
            ).astype(BF16)

    arrived(res.at[0 : 7 * own_rows], t_ss)


def local(
    n,
    n_tp,
    queries,
    keys,
    values,
    query_gain,
    key_gain,
    out_weight,
    residual_in,
    norm_gain,
    gate_weight,
    up_weight,
    down_weight,
):
    tok = queries.shape[0]
    own_rows, d = residual_in.shape
    ff = down_weight.shape[0]
    gk = gate_weight.shape[0]
    ff_pad = -(-ff // HD) * HD
    half = HD // 2
    half_n = n // 2
    inverse = 10000.0 ** (-np.arange(0, half, 2, dtype=np.float32) / half)
    inverse = jnp.asarray(np.tile(np.repeat(inverse, 2), 2)[None].astype(np.float32))
    vmem = pl.BlockSpec(memory_space=pltpu.VMEM)
    dma = pltpu.SemaphoreType.DMA
    scratch = [
        pltpu.VMEM((n, tok, 2 * HD), BF16),
        pltpu.VMEM((tok, HD), BF16),
        pltpu.VMEM((tok, HD), F32),
        pltpu.VMEM((tok, HD), F32),
        pltpu.VMEM((tok, HD), F32),
        pltpu.VMEM((ROWS_ATT, tok), F32),
        pltpu.VMEM((ROWS_ATT, tok), F32),
        pltpu.VMEM((ROWS_ATT, HD), F32),
        pltpu.VMEM((ROWS_ATT, HD), F32),
        pltpu.VMEM((tok // GRID_W, HD), F32),
        pltpu.VMEM((tok // GRID_W, HD), F32),
        pltpu.VMEM((2 * ff_pad, n * gk), BF16),
        pltpu.VMEM((ff, n * HD), BF16),
        pltpu.VMEM(out_weight.shape, BF16),
        pltpu.VMEM((tok, d), BF16),
        pltpu.VMEM((tok, HQ * HD), BF16),
        pltpu.VMEM((tok, d), BF16),
        pltpu.VMEM((own_rows, d), F32),
        pltpu.VMEM((4, ROWS_FF, ff), BF16),
        pltpu.VMEM((ROWS_FF, d), F32),
        pltpu.VMEM((4, own_rows, d), BF16),
        pltpu.VMEM((4, own_rows, d), BF16),
        pltpu.VMEM((4, own_rows, d), F32),
        pltpu.VMEM((6, own_rows, d // 2), BF16),
        pltpu.VMEM((6, own_rows, d // 2), BF16),
        dma,
        dma((half_n + 1,)),
        dma((half_n + 1, 2, 2)),
        dma((half_n + 1, 2)),
        dma((half_n + 1, 2)),
        dma((2, half_n + 1)),
        dma((2, half_n + 1)),
        dma,
        dma,
        dma((12,)),
        dma,
        dma((11,)),
        dma,
        dma((10,)),
    ]
    specs = [vmem] * 12
    specs[6] = pl.BlockSpec(memory_space=pl.ANY)
    return pl.pallas_call(
        functools.partial(layer_kernel, n, n_tp),
        out_shape=jax.ShapeDtypeStruct((own_rows, d), BF16),
        in_specs=specs,
        out_specs=vmem,
        scratch_shapes=scratch,
        compiler_params=pltpu.CompilerParams(
            collective_id=0, has_side_effects=True, vmem_limit_bytes=67043328
        ),
        name="layer",
    )(
        queries,
        keys,
        values,
        query_gain[None],
        key_gain[None],
        inverse,
        out_weight,
        residual_in,
        norm_gain[None],
        gate_weight.T,
        up_weight.T,
        down_weight,
    )


def solution(mesh):
    placed = (
        P(("grp", "sp"), "tp"),
        P(("grp", "sp"), None),
        P(("grp", "sp"), None),
        P(),
        P(),
        P(),
        P(("grp", "sp", "tp"), None),
        P(),
        P("sp", "tp"),
        P("sp", "tp"),
        P("tp", "sp"),
    )
    return jax.shard_map(
        functools.partial(local, mesh.shape["sp"], mesh.shape["tp"]),
        mesh=mesh,
        in_specs=placed,
        out_specs=P(("grp", "sp", "tp"), None),
        check_vma=False,
    )
```

time: 140 us -> 130 us (0.929)
  Pallas kernels: 137 us -> 128 us
    pallas_call x1, Pallas kernels: 137 us -> 128 us  [local(): pl.pallas_call(functools.partial(layer_kernel, n, n_tp), out_shape=jax.Sh...]
where the time goes in v3:
time: 130 us; the launch traced here: 129 us
  Pallas kernels  128 us (98%)
  local copies, waits for them, and re-layouts  1.88 us (1%)
    pallas_call x1, Pallas kernels, local(): pl.pallas_call(functools.partial(layer_kernel, n, n_tp), out_shape=jax.Sh...  128 us

profile of v3, /device:TPU:33, one launch (start us, length us, event | category | flops | bytes accessed | tf_op | source)
XLA Modules:
  0.0 129.4 jit_solution(15921982847735074722)
XLA Ops:
  0.0 127.5 %layer.1 = bf16[128,2048]{1,0:T(8,128)(2,1)} custom-call(bf16[1024,128]{1,0:T(8,128)(2,1)} %q_ref.1, bf16[1024,256]{1,0:T(8,128)(2,1)} %k_ref.1, bf16[1024,256]{1,0:T(8,128)(2,1)} %v_ref.1, f32[1,128]{1,0:T(1,128)} %bitcast.8, f32[1,128]{1,0:T(1,128)} %bitcast.9, f32[1,128]{1,0:T(1,128)} %constant.2.clone.inv_ref, bf16[1024,2048]{1,0:T(8,128)(2,1)} %ow_hbm.1, ...), custom_call_target="tpu_custom_call" | custom-call | tf_op jit(solution)/shard_map/layer/pallas_call | solution.py:774
  127.5 1.9 %copy.14 = bf16[128,2048]{1,0:T(8,128)(2,1)} copy(bf16[128,2048]{1,0:T(8,128)(2,1)} %layer.1) | data formatting | bytes 1048576

commit v4 on v3

--- a/solution.py
+++ b/solution.py
@@ -611,6 +611,7 @@
     pump()
     taken(3)
     project(3)
+    pump()
     w_taken()
 
     half_d = d // 2
@@ -663,7 +664,6 @@
                 yk[3, :, cols[c]] = both(3, c) + mid[:, cols[c]]
 
     units(0)
-    pump()
     units(1)
     units(2)
     pump()

time: 130 us -> 127 us (0.977)
  Pallas kernels: 128 us -> 125 us
    pallas_call x1, Pallas kernels: 128 us -> 125 us  [local(): pl.pallas_call(functools.partial(layer_kernel, n, n_tp), out_shape=jax.Sh...]
where the time goes in v4:
time: 127 us
  Pallas kernels  125 us (98%)
  local copies, waits for them, and re-layouts  1.88 us (1%)
    pallas_call x1, Pallas kernels, local(): pl.pallas_call(functools.partial(layer_kernel, n, n_tp), out_shape=jax.Sh...  125 us

profile of v4, /device:TPU:33, one launch (start us, length us, event | category | flops | bytes accessed | tf_op | source)
XLA Modules:
  0.0 126.6 jit_solution(335469742556596206)
XLA Ops:
  0.0 124.7 %layer.1 = bf16[128,2048]{1,0:T(8,128)(2,1)} custom-call(bf16[1024,128]{1,0:T(8,128)(2,1)} %q_ref.1, bf16[1024,256]{1,0:T(8,128)(2,1)} %k_ref.1, bf16[1024,256]{1,0:T(8,128)(2,1)} %v_ref.1, f32[1,128]{1,0:T(1,128)} %bitcast.8, f32[1,128]{1,0:T(1,128)} %bitcast.9, f32[1,128]{1,0:T(1,128)} %constant.2.clone.inv_ref, bf16[1024,2048]{1,0:T(8,128)(2,1)} %ow_hbm.1, ...), custom_call_target="tpu_custom_call" | custom-call | tf_op jit(solution)/shard_map/layer/pallas_call | solution.py:774
  124.7 1.9 %copy.14 = bf16[128,2048]{1,0:T(8,128)(2,1)} copy(bf16[128,2048]{1,0:T(8,128)(2,1)} %layer.1) | data formatting | bytes 1048576
